TPU v7x, 128 devices: a whole 4x4x4 slice. The times are simulated.
128 devices in a mesh: ep: 64 (over z, y, x), tp: 2 (over core).
Axes of the slice: x: 4, y: 4, z: 4, core: 2. Of those that a mesh axis runs over, the one named last changes fastest.
Arguments:
- stream: bfloat16 [2048, 2048], P('ep'), may hold values from -6 to 6
- mixer_gain: float32 [2048], replicated, may hold values from 0.1 to 1.9
- gate_proj: bfloat16 [2048, 1024], P(None, 'tp'), may hold values from -0.125 to 0.125
- input_proj: bfloat16 [2048, 1024], P(None, 'tp'), may hold values from -0.125 to 0.125
- state_maps: bfloat16 [2, 2048, 256], P(None, None, 'tp'), may hold values from -0.125 to 0.125
- step_proj: bfloat16 [2048, 16], P(None, 'tp'), may hold values from -0.125 to 0.125
- step_bias: float32 [16], P('tp'), may hold values from -3 to 0.5
- decay_rate: float32 [16], P('tp'), may hold values from 0.05 to 4
- input_taps: float32 [4, 1024], P(None, 'tp'), may hold values from -3 to 3
- map_taps: float32 [2, 4, 256], P(None, None, 'tp'), may hold values from -3 to 3
- input_past: bfloat16 [2048, 3, 1024], P('ep', None, 'tp'), may hold values from -6 to 6
- map_past: bfloat16 [2048, 2, 3, 256], P('ep', None, None, 'tp'), may hold values from -6 to 6
- head_state: float32 [2048, 16, 4096], P('ep', 'tp'), may hold values from -1.6 to 1.6
- skip_gain: float32 [16], P('tp'), may hold values from 0 to 2
- inner_gain: float32 [1024], P('tp'), may hold values from 0.1 to 1.9
- mixer_out: bfloat16 [1024, 2048], P('tp'), may hold values from -0.1875 to 0.1875
- channel_gain: float32 [2048], replicated, may hold values from 0.1 to 1.9
- expert_ids: int32 [2048, 2], P('ep'), may hold values from 0 to 7, all different within a row; in each aligned block of 32 rows (0 to 31, 32 to 63, ...) at most 12 rows name the same one
- expert_weight: float32 [2048, 2], P('ep'), may hold values from 0.2 to 1
- expert_gate: bfloat16 [2048, 57344], P(None, ('ep', 'tp')), may hold values from -0.125 to 0.125
- expert_up: bfloat16 [2048, 57344], P(None, ('ep', 'tp')), may hold values from -0.125 to 0.125
- expert_down: bfloat16 [57344, 2048], P(('ep', 'tp')), may hold values from -0.0625 to 0.0625
- dense_gate: bfloat16 [2048, 5632], P('tp', 'ep'), may hold values from -0.125 to 0.125
- dense_up: bfloat16 [2048, 5632], P('tp', 'ep'), may hold values from -0.125 to 0.125
- dense_down: bfloat16 [5632, 2048], P('ep', 'tp'), may hold values from -0.078125 to 0.078125
- dense_mix: float32 [2048], P('tp'), may hold values from -2 to 2
Outputs:
- stream_out: bfloat16 [2048, 2048], P('ep', 'tp')
- state_out: float32 [2048, 16, 4096], P('ep', 'tp')
Inputs may be any that keep to these rules, and one draw needn't show every extreme that they name: `expert_ids`: each row names 2 different experts. In each aligned block of 32 rows no expert is named by more than 12 rows, and in some block one expert is named by exactly 12 rows.
All inputs are finite; a program needn't handle non-finite values.
Results may differ from a plain program's by a relative error of at most 0.015.
Values may be sent and summed in bfloat16 or wider, within the bound.
A program may use at most 128 MiB of HBM per device.

v0:
```python
import jax
import jax.numpy as jnp
from jax import lax
from jax.sharding import PartitionSpec as P

HEAD = 64
HEADS = 16
GROUPS = 4
NSTATE = 64
EXPERTS = 8
TOP_K = 2
CAP = 12


EPS = 1e-06


def copy_for_each(array, axis):
    devices = lax.axis_size(axis)
    return lax.all_to_all(
        jnp.broadcast_to(array[None], (devices, *array.shape)), axis, 0, 0, tiled=True
    )


def over_copies(array, axis):
    return copy_for_each(array, axis).astype(jnp.float32).sum(axis=0)


def in_blocks(array, dim, devices):
    before, after = (array.shape[:dim], array.shape[dim + 1 :])
    return jnp.moveaxis(array.reshape(*before, devices, -1, *after), dim, 0)


def summed_on_arrival(array, axis, dim):
    devices = lax.axis_size(axis)
    blocks = lax.all_to_all(in_blocks(array, dim, devices), axis, 0, 0, tiled=True)
    return jnp.sum(blocks.astype(jnp.float32), axis=0)


def side_by_side(arrays, axis, dim, along):
    widths = [a.shape[along] for a in arrays]
    both = jnp.concatenate(arrays, axis=along)
    out = lax.all_gather(both, axis, axis=dim, tiled=True)
    return tuple(jnp.split(out, [sum(widths[:k]) for k in range(1, len(widths))], axis=along))


def rms_scale(values):
    return values * lax.rsqrt(jnp.mean(values * values, axis=-1, keepdims=True) + EPS)


def short_conv(past_rows, newest, tap_weights, along):
    window = jnp.concatenate([past_rows, jnp.expand_dims(newest, along)], axis=along).astype(
        jnp.float32
    )
    return jax.nn.silu(jnp.sum(window * tap_weights, axis=along))


def mix_heads(
    stream,
    mixer_gain,
    gate_proj,
    input_proj,
    state_maps,
    step_proj,
    step_bias,
    decay_rate,
    input_taps,
    map_taps,
    input_past,
    map_past,
    head_state,
    skip_gain,
    inner_gain,
):
    row_count = stream.shape[0]
    normed = (rms_scale(stream.astype(jnp.float32)) * mixer_gain).astype(jnp.bfloat16)
    gate_in = jnp.dot(normed, gate_proj, preferred_element_type=jnp.float32).astype(jnp.bfloat16)
    input_new = jnp.dot(normed, input_proj, preferred_element_type=jnp.float32).astype(jnp.bfloat16)
    map_new = jnp.stack(
        [
            jnp.dot(normed, state_maps[0], preferred_element_type=jnp.float32),
            jnp.dot(normed, state_maps[1], preferred_element_type=jnp.float32),
        ],
        axis=1,
    ).astype(jnp.bfloat16)
    step_size = jax.nn.softplus(
        jnp.dot(normed, step_proj, preferred_element_type=jnp.float32) + step_bias
    )
    conv_in = short_conv(input_past, input_new, input_taps, 1)
    conv_map = short_conv(map_past, map_new, map_taps, 2)
    head_count = step_size.shape[1]
    per_group = HEADS // GROUPS
    group_count = head_count // per_group
    write_map = jnp.repeat(
        conv_map[:, 0].reshape(row_count, group_count, NSTATE), per_group, axis=1
    )
    read_map = jnp.repeat(conv_map[:, 1].reshape(row_count, group_count, NSTATE), per_group, axis=1)
    values = conv_in.reshape(row_count, head_count, HEAD)
    decay_now = jnp.exp(-decay_rate * step_size)
    state_old = head_state.reshape(row_count, head_count, HEAD, NSTATE)
    state_new = (
        decay_now[:, :, None, None] * state_old
        + (step_size[:, :, None] * values)[:, :, :, None] * write_map[:, :, None, :]
    )
    gated = jnp.sum(state_new * read_map[:, :, None, :], axis=3) + skip_gain[:, None] * values
    gated = gated.reshape(row_count, head_count * HEAD) * jax.nn.silu(gate_in.astype(jnp.float32))
    inner_out = (
        rms_scale(gated.reshape(row_count, group_count, -1)).reshape(row_count, -1) * inner_gain
    )
    return (inner_out.astype(jnp.bfloat16), state_new.reshape(row_count, head_count, HEAD * NSTATE))


def local(
    stream,
    mixer_gain,
    gate_proj,
    input_proj,
    state_maps,
    step_proj,
    step_bias,
    decay_rate,
    input_taps,
    map_taps,
    input_past,
    map_past,
    head_state,
    skip_gain,
    inner_gain,
    mixer_out,
    channel_gain,
    expert_ids,
    expert_weight,
    expert_gate,
    expert_up,
    expert_down,
    dense_gate,
    dense_up,
    dense_down,
    dense_mix,
):
    inner_out, state_out = mix_heads(
        stream,
        mixer_gain,
        gate_proj,
        input_proj,
        state_maps,
        step_proj,
        step_bias,
        decay_rate,
        input_taps,
        map_taps,
        input_past,
        map_past,
        head_state,
        skip_gain,
        inner_gain,
    )
    partial_out = jnp.dot(inner_out, mixer_out, preferred_element_type=jnp.float32)
    mixed = over_copies(partial_out.astype(jnp.bfloat16), "tp").astype(jnp.float32)
    hidden_mid = stream.astype(jnp.float32) + mixed
    ffn_in = (rms_scale(hidden_mid) * channel_gain).astype(jnp.bfloat16)
    row_count, feature_count = ffn_in.shape
    half_width = feature_count // lax.axis_size("tp")
    offset = lax.axis_index("tp") * half_width
    own_half = lax.dynamic_slice_in_dim(ffn_in, offset, half_width, 1)
    kept = lax.dynamic_slice_in_dim(hidden_mid, offset, half_width, 1)
    expert_span = lax.axis_size("ep") // EXPERTS
    flat_ids = expert_ids.reshape(-1)
    hit_table = (flat_ids[:, None] == jnp.arange(EXPERTS, dtype=jnp.int32)[None, :]).astype(
        jnp.int32
    )
    slot_rank = jnp.sum(jnp.cumsum(hit_table, axis=0) * hit_table, axis=1) - 1
    slot_index = flat_ids * CAP + slot_rank
    slot_table = (
        slot_index[:, None] == jnp.arange(EXPERTS * CAP, dtype=jnp.int32)[None, :]
    ).astype(jnp.float32)
    slot_table = slot_table.reshape(row_count, TOP_K, EXPERTS * CAP)
    chosen = jnp.sum(slot_table, axis=1).astype(jnp.bfloat16)
    outgoing = jnp.dot(chosen.T, ffn_in, preferred_element_type=jnp.float32).astype(jnp.bfloat16)
    outgoing = jnp.repeat(outgoing.reshape(EXPERTS, CAP, feature_count), expert_span, axis=0)
    received = lax.all_to_all(outgoing, "ep", split_axis=0, concat_axis=0, tiled=True)
    sources, item_count, width_in = received.shape
    flat_rows = received.reshape(sources * item_count, width_in)
    gate_val = jnp.dot(flat_rows, expert_gate, preferred_element_type=jnp.float32)
    up_val = jnp.dot(flat_rows, expert_up, preferred_element_type=jnp.float32)
    act = (jax.nn.silu(gate_val) * up_val).astype(jnp.bfloat16)
    share = jnp.dot(act, expert_down, preferred_element_type=jnp.float32).reshape(
        sources, item_count, width_in
    )
    halves = summed_on_arrival(share.astype(jnp.bfloat16), "tp", 2)
    piece = lax.all_gather(own_half, "ep", axis=0, tiled=True)
    gathered = jnp.concatenate(
        [
            jnp.dot(piece, dense_gate, preferred_element_type=jnp.float32),
            jnp.dot(piece, dense_up, preferred_element_type=jnp.float32),
        ],
        axis=1,
    )
    summed = over_copies(gathered.astype(jnp.bfloat16), "tp").astype(jnp.float32)
    unit_count = dense_gate.shape[1]
    dense_act = (jax.nn.silu(summed[:, :unit_count]) * summed[:, unit_count:]).astype(jnp.bfloat16)
    mix_scale = jax.nn.sigmoid(dense_mix)
    table_ids, table_weight = side_by_side(
        (expert_ids.astype(jnp.float32), expert_weight), "ep", 0, 1
    )
    sources = lax.axis_size("ep")
    own_expert = lax.axis_index("ep") // expert_span
    source_ids = table_ids.astype(jnp.int32).reshape(sources, row_count * TOP_K)
    matched = (source_ids == own_expert).astype(jnp.int32)
    source_rank = jnp.cumsum(matched, axis=1) - 1
    onehot = (
        (source_rank[:, :, None] == jnp.arange(CAP, dtype=jnp.int32)[None, None, :])
        * matched[:, :, None]
    ).astype(jnp.float32)
    weighted = onehot * table_weight.reshape(sources, row_count * TOP_K, 1)
    combine = jnp.sum(weighted.reshape(sources, row_count, TOP_K, CAP), axis=2)
    dense_part = jnp.dot(dense_act, dense_down, preferred_element_type=jnp.float32) * mix_scale
    routed_part = jnp.einsum("bsc,bcd->bsd", combine, halves, precision=lax.Precision.HIGHEST)
    updated = kept + summed_on_arrival(
        (dense_part + routed_part.reshape(row_count * lax.axis_size("ep"), -1)).astype(
            jnp.bfloat16
        ),
        "ep",
        0,
    )
    return (updated.astype(jnp.bfloat16), state_out)


def solution(mesh):
    placed = (
        P("ep", None),
        P(),
        P(None, "tp"),
        P(None, "tp"),
        P(None, None, "tp"),
        P(None, "tp"),
        P("tp"),
        P("tp"),
        P(None, "tp"),
        P(None, None, "tp"),
        P("ep", None, "tp"),
        P("ep", None, None, "tp"),
        P("ep", "tp", None),
        P("tp"),
        P("tp"),
        P("tp", None),
        P(),
        P("ep", None),
        P("ep", None),
        P(None, ("ep", "tp")),
        P(None, ("ep", "tp")),
        P(("ep", "tp"), None),
        P("tp", "ep"),
        P("tp", "ep"),
        P("ep", "tp"),
        P("tp"),
    )
    return jax.shard_map(
        local,
        mesh=mesh,
        in_specs=placed,
        out_specs=(P("ep", "tp"), P("ep", "tp", None)),
        check_vma=False,
    )
```

profile of v0, /device:TPU:0, one launch (start us, length us, event | category | flops | bytes accessed | tf_op | source)
XLA Modules:
  0.0 427.2 jit_solution(4112670751748664089)
XLA Ops:
  7.2 1.2 fusion.15
  8.4 1.4 fusion.6
  9.8 1.4 fusion.7
  13.4 1.2 multiply_exponential_fusion
  15.9 2.2 fusion.5
  18.3 7.9 %reshape.200 = f32[32,8,64,64]{3,2,1,0:T(8,128)} reshape(f32[32,8,4096]{2,1,0:T(8,128)} %param.38) | data formatting | bytes 8388608 | tf_op jit(solution)/shard_map/reshape | solution.py:100
  26.3 8.6 %broadcast_multiply_fusion = (f32[32,8,64,64]{3,2,1,0:T(8,128)}, f32[32,8,64]{2,1,0:T(8,128)S(1)}) fusion(f32[32,8,64]{2,1,0:T(8,128)S(1)} %bitcast.60, f32[32,8,64]{2,1,0:T(8,128)S(1)} %multiply_multiply_fusion, f32[32,8,64]{2,1,0:T(8,128)S(1)} %bitcast.59, f32[32,8,64,64]{3,2,1,0:T(8,128)} %reshape.200, f32[32,8]{1,0:T(8,128)S(1)} %copy.132), kind=kLoop, calls=%fused_computation.8 | loop fusion | flops 5226496 | bytes 8651776 | tf_op jit(solution)/shard_map/mul | solution.py:103
  35.1 2.1 fusion.28
  38.8 3.4 all-to-all-start
  42.3 1.5 all-to-all-done
  46.0 2.5 broadcast_in_dim.17
  48.5 11.9 %all-to-all-start.2 = ((bf16[64,12,2048]{2,1,0:T(8,128)(2,1)}), bf16[64,12,2048]{2,1,0:T(8,128)(2,1)}, u32[]{:S(2)}, u32[]{:S(2)}) async-start(bf16[64,12,2048]{2,1,0:T(8,128)(2,1)} %bitcast.57), calls=%async_computation.2 | async-start | bytes 8388608 | tf_op jit(solution)/shard_map/all_to_all | solution.py:181
  60.5 214.5 %all-gather = f32[64,32,4]{1,2,0:T(4,128)S(1)} all-gather(f32[1,32,4]{1,2,0:T(4,128)S(1)} %maximum_bitcast_fusion), channel_id=1, replica_groups=mesh['ep'=64,'tp'=2] {'ep'}, dimensions={0}, use_global_device_ids=true | all-gather | bytes 33280 | tf_op jit(solution)/shard_map/all_gather | solution.py:43
  276.6 2.0 copy.138
  278.5 15.4 %fusion.29 = s32[64,64,1]{2,0,1:T(8,128)S(1)} fusion(s32[64,64,1]{2,0,1:T(8,128)S(1)} %copy.138), kind=kOutput, calls=%fused_computation.79 | output fusion | flops 258048 | bytes 32768 | tf_op jit(solution)/shard_map/jit(cumsum)/reduce_window_sum | solution.py:210
  294.0 1.2 add_reduce_fusion
  295.5 6.2 %reshape.203 = bf16[768,2048]{1,0:T(8,128)(2,1)} reshape(bf16[64,12,2048]{2,1,0:T(8,128)(2,1)} %all-to-all-done.2) | data formatting | bytes 6291456 | tf_op jit(solution)/shard_map/reshape | solution.py:183
  301.7 4.1 fusion.30
  305.8 9.0 %convolution_convert_fusion = bf16[768,2048]{1,0:T(8,128)(2,1)} fusion(bf16[448,2048]{1,0:T(8,128)(2,1)} %param.47, bf16[768,2048]{1,0:T(8,128)(2,1)} %reshape.203, bf16[2048,448]{0,1:T(8,128)(2,1)} %param.46, f32[768,448]{0,1:T(8,128)S(1)} %fusion.30), kind=kOutput, calls=%fused_computation.9 | convolution fusion | flops 2822209536 | bytes 11337728 | tf_op jit(solution)/shard_map/dot_general | solution.py:187
  314.8 6.1 %convert_element_type.145 = bf16[64,12,2,1024]{3,2,1,0:T(2,128)(2,1)} reshape(bf16[768,2048]{1,0:T(8,128)(2,1)} %convolution_convert_fusion) | data formatting | bytes 6291456 | tf_op jit(solution)/shard_map/convert_element_type | solution.py:190
  320.9 3.6 copy.152
  324.5 6.3 %all_to_all.25 = bf16[2,64,12,1024]{3,1,2,0:T(8,128)(2,1)S(1)} all-to-all(bf16[2,64,12,1024]{3,1,2,0:T(8,128)(2,1)S(1)} %bitcast.58), channel_id=1, replica_groups=mesh['ep'=64,'tp'=2] {'tp'}, dimensions={0} | all-to-all | bytes 6291456 | tf_op jit(solution)/shard_map/all_to_all | solution.py:36
  331.5 10.2 %fusion.1 = f32[64,32,1024]{2,1,0:T(8,128)} fusion(f32[64,32,12]{1,2,0:T(8,128)S(1)} %copy.145, f32[64,12,1024]{2,0,1:T(8,128)S(1)} %convert_reduce_fusion.1), kind=kOutput, calls=%fused_computation.5 | convolution fusion | flops 301989888 | bytes 11632640 | tf_op jit(solution)/shard_map/bsc,bcd->bsd/dot_general | solution.py:218
  341.7 3.7 convolution_convert_fusion.2
  345.5 1.4 convolution_convert_fusion.3
  347.1 5.2 %all_to_all.26 = bf16[2,2048,176]{1,2,0:T(8,128)(2,1)S(1)} all-to-all(bf16[2,2048,176]{1,2,0:T(8,128)(2,1)S(1)} %broadcast_in_dim.16), channel_id=1, replica_groups=mesh['ep'=64,'tp'=2] {'tp'}, dimensions={0} | all-to-all | bytes 2883584 | tf_op jit(solution)/shard_map/all_to_all | solution.py:20
  352.6 3.3 fusion
  356.0 5.9 %all-to-all-start.4 = ((bf16[64,32,1024]{2,1,0:T(8,128)(2,1)}), bf16[64,32,1024]{2,1,0:T(8,128)(2,1)}, u32[]{:S(2)}, u32[]{:S(2)}) async-start(bf16[64,32,1024]{2,1,0:T(8,128)(2,1)} %bitcast.56), calls=%async_computation.4 | async-start | bytes 8388608 | tf_op jit(solution)/shard_map/all_to_all | solution.py:36
  361.9 7.9 %mul.293 = f32[32,8,4096]{2,1,0:T(8,128)} reshape(f32[32,8,64,64]{3,2,1,0:T(8,128)} %get-tuple-element.6) | data formatting | bytes 8388608 | tf_op jit(solution)/shard_map/mul | solution.py:103
  369.8 6.7 %multiply_add_fusion = f32[32,8,4096]{2,1,0:T(8,128)} fusion(f32[32,8,4096]{2,1,0:T(8,128)} %mul.293, f32[32,8,4096]{2,1,0:T(8,128)} %param.38, f32[32,8]{1,0:T(8,128)S(1)} %copy.132), kind=kLoop, calls=%fused_computation.7 | loop fusion | flops 2097152 | bytes 12583936 | tf_op jit(solution)/shard_map/add | solution.py:102
  376.5 40.2 %all-to-all-done.4 = bf16[64,32,1024]{2,1,0:T(8,128)(2,1)} async-done(((bf16[64,32,1024]{2,1,0:T(8,128)(2,1)}), bf16[64,32,1024]{2,1,0:T(8,128)(2,1)}, u32[]{:S(2)}, u32[]{:S(2)}) %all-to-all-start.4) | async-done | bytes 4194336 | tf_op jit(solution)/shard_map/all_to_all | solution.py:36
  416.7 3.0 convert_reduce_fusion
  (103 shorter events, 11.4 us)
Async XLA Ops:
  7.2 30.4 %copy-start = (bf16[512,2048]{1,0:T(8,128)(2,1)S(1)}, bf16[512,2048]{1,0:T(8,128)(2,1)}, u32[]{:S(2)}) copy-start(bf16[512,2048]{1,0:T(8,128)(2,1)} %param.41) | copy-start | bytes 6291460
  7.2 11.0 %copy-start.7 = (bf16[32,3,512]{2,0,1:T(8,128)(2,1)S(1)}, bf16[32,3,512]{2,0,1:T(8,128)(2,1)}, u32[]{:S(2)}) copy-start(bf16[32,3,512]{2,0,1:T(8,128)(2,1)} %param.36) | copy-start | bytes 294916
  7.2 11.0 %copy-start.9 = (f32[4,512]{1,0:T(4,128)S(1)}, f32[4,512]{1,0:T(4,128)}, u32[]{:S(2)}) copy-start(f32[4,512]{1,0:T(4,128)} %param.34) | copy-start | bytes 24580
  26.3 8.8 %copy-start.3 = (bf16[32,2048]{1,0:T(8,128)(2,1)S(1)}, bf16[32,2048]{1,0:T(8,128)(2,1)}, u32[]{:S(2)}) copy-start(bf16[32,2048]{1,0:T(8,128)(2,1)} %param.26) | copy-start | bytes 393220
  26.3 8.8 %copy-start.8 = (f32[2048]{0:T(1024)S(1)}, f32[2048]{0:T(1024)}, u32[]{:S(2)}) copy-start(f32[2048]{0:T(1024)} %param.27) | copy-start | bytes 24580
  35.0 2.6 copy-start.13
  35.1 8.9 %copy-start.10 = (f32[2048]{0:T(1024)S(1)}, f32[2048]{0:T(1024)}, u32[]{:S(2)}) copy-start(f32[2048]{0:T(1024)} %param.42) | copy-start | bytes 24580
  37.3 7.5 %copy-start.12 = (s32[32,2]{0,1:T(2,128)S(1)}, s32[32,2]{0,1:T(2,128)}, u32[]{:S(2)}) copy-start(s32[32,2]{0,1:T(2,128)} %param.43) | copy-start | bytes 772
  38.8 5.0 %all-to-all-start = ((bf16[2,32,2048]{2,1,0:T(8,128)(2,1)}), bf16[2,32,2048]{2,1,0:T(8,128)(2,1)S(1)}, u32[]{:S(2)}, u32[]{:S(2)}) async-start(bf16[2,32,2048]{2,1,0:T(8,128)(2,1)} %broadcast_in_dim.15), calls=%async_computation | async-start | bytes 524288 | tf_op jit(solution)/shard_map/all_to_all | solution.py:20
  42.2 299.5 %all-gather.3.cloned.1.call-start = ((), (), s32[]{:S(2)}) async-start(), calls=%async_computation.5 | async-start | bytes 4259840 | tf_op jit(solution)/shard_map/all_gather | solution.py:191
  48.5 11.9 %copy-start.14 = (f32[32,2]{0,1:T(2,128)S(1)}, f32[32,2]{0,1:T(2,128)}, u32[]{:S(2)}) copy-start(f32[32,2]{0,1:T(2,128)} %param.44) | copy-start | bytes 772
  48.5 247.0 %all-to-all-start.2 = ((bf16[64,12,2048]{2,1,0:T(8,128)(2,1)}), bf16[64,12,2048]{2,1,0:T(8,128)(2,1)}, u32[]{:S(2)}, u32[]{:S(2)}) async-start(bf16[64,12,2048]{2,1,0:T(8,128)(2,1)} %bitcast.57), calls=%async_computation.2 | async-start | bytes 8388608 | tf_op jit(solution)/shard_map/all_to_all | solution.py:181
  278.5 17.0 %copy-start.11 = (f32[1024]{0:T(1024)S(1)}, f32[1024]{0:T(1024)}, u32[]{:S(2)}) copy-start(f32[1024]{0:T(1024)} %param.51) | copy-start | bytes 12292
  331.5 10.2 %copy-start.4 = (bf16[1024,88]{0,1:T(8,128)(2,1)S(1)}, bf16[1024,88]{0,1:T(8,128)(2,1)}, u32[]{:S(2)}) copy-start(bf16[1024,88]{0,1:T(8,128)(2,1)} %param.49) | copy-start | bytes 540676
  341.7 3.8 copy-start.5
  341.7 3.8 copy-start.2
  345.5 7.1 %slice-start = ((s8[8388608]{0:T(1024)(128)(4,1)}), s8[4194304]{0:T(1024)(128)(4,1)S(1)}, s32[]{:S(2)}) async-start(s8[8388608]{0:T(1024)(128)(4,1)} %bitcast.54), calls=%async_computation.6 | async-start | bytes 8388608
  347.0 5.6 %slice-start.1 = ((s8[8388608]{0:T(1024)(128)(4,1)}), s8[4194304]{0:T(1024)(128)(4,1)S(1)}, s32[]{:S(2)}) async-start(s8[8388608]{0:T(1024)(128)(4,1)} %bitcast.54), calls=%async_computation.7 | async-start | bytes 8388608
  347.1 5.5 %copy-start.6 = (bf16[88,1024]{1,0:T(8,128)(2,1)S(1)}, bf16[88,1024]{1,0:T(8,128)(2,1)}, u32[]{:S(2)}) copy-start(bf16[88,1024]{1,0:T(8,128)(2,1)} %param.50) | copy-start | bytes 540676
  356.0 60.7 %all-to-all-start.4 = ((bf16[64,32,1024]{2,1,0:T(8,128)(2,1)}), bf16[64,32,1024]{2,1,0:T(8,128)(2,1)}, u32[]{:S(2)}, u32[]{:S(2)}) async-start(bf16[64,32,1024]{2,1,0:T(8,128)(2,1)} %bitcast.56), calls=%async_computation.4 | async-start | bytes 8388608 | tf_op jit(solution)/shard_map/all_to_all | solution.py:36
  369.8 50.6 %copy-start.1 = (bf16[512,2048]{1,0:T(8,128)(2,1)S(1)}, bf16[512,2048]{1,0:T(8,128)(2,1)}, u32[]{:S(2)}) copy-start(bf16[512,2048]{1,0:T(8,128)(2,1)} %param.41) | copy-start | bytes 6291460
Sparse Core Ops, SparseCore 0:
  46.5 109.1 all-gather.2
where the time goes:
time: 428 us; the launch traced here: 427 us
  blocking collectives  226 us (53%)
  local copies, waits for them, and re-layouts  42.3 us (10%)
  waiting for transfers between devices  41.7 us (10%)
  matrix products  40.7 us (10%)
  other arithmetic  40.6 us (9%)
  starting transfers between devices  21.3 us (5%)
  between operations  14.7 us (3%)
    all_gather x1, blocking collectives, side_by_side(): out = lax.all_gather(both, axis, axis=dim, tiled=True)  215 us
    all_to_all x1, waiting for transfers between devices, summed_on_arrival(): lax.all_to_all(in_blocks(array, dim, devices), axis, 0, 0, tiled=True)  40.2 us
    another operation x1, other arithmetic, local(): source_rank = jnp.cumsum(matched, axis=1) - 1  15.4 us
    all_to_all x1, starting transfers between devices, local(): lax.all_to_all(outgoing, 'ep', split_axis=0, concat_axis=0, tiled=True)  11.9 us
    dot_general x1, matrix products, local(): jnp.einsum('bsc,bcd->bsd', combine, halves, precision=lax.Precision.HIGHEST)  10.2 us
    convert_element_type x2, local copies, waits for them, and re-layouts, local(): halves = summed_on_arrival(share.astype(jnp.bfloat16), 'tp', 2)  9.74 us
    dot_general x1, matrix products, local(): jnp.dot(act, expert_down, preferred_element_type=jnp.float32)  8.98 us
    mul x1, other arithmetic, mix_heads(): (step_size[:, :, None] * values)[:, :, :, None] * write_map[:, :, None, :]  8.65 us
  transfers between devices with their start and end apart: 4, of which 2 were waited for; matrix products, arithmetic and copies ran while one was open for 18% of the time, Pallas kernels for 0%

commit v1 on v0

v1 whole, which is shorter than its diff:
```python
import functools

import jax
import jax.numpy as jnp
from jax import lax
from jax.experimental import pallas as pl
from jax.experimental.pallas import tpu as pltpu
from jax.sharding import PartitionSpec as P

EPS = 1e-06
MESH = pl.DeviceIdType.MESH
F32 = jnp.float32
BF16 = jnp.bfloat16
VMEM = pltpu.VMEM
ANY = pl.ANY

HEADS = 8
ROWS = 32
EXPERTS = 8
CAP = 12
CHUNKS = 8
CHUNK = 512
GROUPS = 8
GROUP_ROWS = 256
SLOTS = 96
HALF = 1024
HIDDEN = 448
HPAD = 512
DENSE = 88

WIDTHS = (384, 384, 256)
STARTS = (0, 384, 768)
BLOCK_ROWS = (32, 32, 48)
ORDERS = ((2, 1, 0), (1, 0, 2), (0, 2, 1))


def dot(a, b):
    return jnp.dot(a, b, preferred_element_type=F32)


def dot_nt(a, b):
    return lax.dot_general(a, b, (((1,), (1,)), ((), ())), preferred_element_type=F32)


def dot_tn(a, b):
    return lax.dot_general(a, b, (((0,), (0,)), ((), ())), preferred_element_type=F32)


def silu(v):
    return v / (1.0 + jnp.exp(-v))


def rms(v):
    return v * lax.rsqrt(jnp.mean(v * v, axis=-1, keepdims=True) + EPS)


def split(v):
    high = v.astype(BF16)
    return high, (v - high.astype(F32)).astype(BF16)


def mixer_kernel(
    stream,
    mixer_gain,
    step_t,
    bias,
    decay,
    skip,
    input_taps,
    map_taps,
    input_past,
    map_past,
    inner_gain,
    ids,
    weights,
    gate_hbm,
    input_hbm,
    maps_hbm,
    out_hbm,
    state_hbm,
    state_out,
    partial,
    meta,
    gate_w,
    input_w,
    maps_w,
    out_w,
    old,
    new,
    dec,
    write,
    read,
    xs_high,
    xs_low,
    tmp,
    y,
    sems,
):
    loads = [
        pltpu.make_async_copy(input_hbm, input_w, sems.at[0]),
        pltpu.make_async_copy(maps_hbm, maps_w, sems.at[1]),
        pltpu.make_async_copy(gate_hbm, gate_w, sems.at[2]),
        pltpu.make_async_copy(out_hbm, out_w, sems.at[3]),
    ]

    def load_state(t):
        cols = pl.ds(pl.multiple_of(t * CHUNK, CHUNK), CHUNK)
        return pltpu.make_async_copy(state_hbm.at[:, cols], old.at[t], sems.at[4 + t])

    def store_state(t):
        cols = pl.ds(pl.multiple_of(t * CHUNK, CHUNK), CHUNK)
        return pltpu.make_async_copy(
            new.at[t], state_out.at[:, cols], sems.at[4 + CHUNKS + t]
        )

    loads[0].start()
    loads[1].start()
    for t in range(CHUNKS):
        load_state(t).start()
    loads[2].start()
    loads[3].start()

    normed = (rms(stream[...].astype(F32)) * mixer_gain[...]).astype(BF16)
    steps = dot_nt(normed, step_t[...])

    expert_of = lax.broadcasted_iota(jnp.int32, (EXPERTS, ROWS), 0)
    hit0 = (ids[0:1, :] == expert_of).astype(F32)
    hit1 = (ids[1:2, :] == expert_of).astype(F32)
    member = hit0 + hit1
    upper = (
        lax.broadcasted_iota(jnp.int32, (ROWS, ROWS), 0)
        <= lax.broadcasted_iota(jnp.int32, (ROWS, ROWS), 1)
    ).astype(BF16)
    rank = dot(member.astype(BF16), upper) * member
    weight = hit0 * weights[0:1, :] + hit1 * weights[1:2, :]
    w_high = weight.astype(BF16).astype(F32)
    w_low = weight - w_high
    table = jnp.concatenate(
        [rank, w_high, w_low, jnp.zeros((104, ROWS), F32)], axis=0
    ).astype(BF16)
    eye = (
        lax.broadcasted_iota(jnp.int32, (ROWS, ROWS), 0)
        == lax.broadcasted_iota(jnp.int32, (ROWS, ROWS), 1)
    ).astype(BF16)
    by_row = dot_nt(eye, table)
    meta[...] = jnp.concatenate([by_row[0:16], by_row[16:32]], axis=1).astype(BF16)

    loads[0].wait()
    newest = dot(normed, input_w[...]).astype(BF16).astype(F32)
    conv = newest * input_taps[3:4, :]
    for t in range(3):
        conv = conv + input_past[t].astype(F32) * input_taps[t : t + 1, :]
    conv = silu(conv)

    loads[1].wait()
    conv_maps = []
    for m in range(2):
        new_map = dot(normed, maps_w[m]).astype(BF16).astype(F32)
        acc = new_map * map_taps[m, 3:4, :]
        for t in range(3):
            acc = acc + map_past[3 * m + t].astype(F32) * map_taps[m, t : t + 1, :]
        conv_maps.append(silu(acc))

    lane = lax.broadcasted_iota(jnp.int32, (ROWS, 128), 1)
    low_half = lane < 64

    def both_halves(v):
        turned = pltpu.roll(v, 64, 1)
        return jnp.where(low_half, v, turned), jnp.where(low_half, turned, v)

    write_by_group = both_halves(conv_maps[0])
    read_by_group = both_halves(conv_maps[1])
    for h in range(HEADS):
        rows = pl.ds(h, ROWS, stride=HEADS)
        v = jnp.broadcast_to(steps[:, h : h + 1], (ROWS, 128)) + bias[h]
        step = jnp.maximum(v, 0.0) + jnp.log1p(jnp.exp(-jnp.abs(v)))
        dec[rows, :] = jnp.exp(-decay[h] * step)
        pair = conv[:, 128 * (h // 2) : 128 * (h // 2) + 128]
        mine = low_half if h % 2 == 0 else jnp.logical_not(low_half)
        tmp[rows, :] = jnp.where(mine, step * pair, 0.0)
        write[rows, :] = write_by_group[h // 4]
        read[rows, :] = read_by_group[h // 4]
    high, low = split(tmp[...])
    xs_high[...] = high
    xs_low[...] = low
    y[...] = jnp.zeros_like(y)

    slot = lax.broadcasted_iota(jnp.int32, (128, CHUNK), 0) % 64
    place = lax.broadcasted_iota(jnp.int32, (128, CHUNK), 1) // 64

    def chunk_step(t, carry):
        spread = (slot == place + 8 * t).astype(F32).astype(BF16)
        load_state(t).wait()
        values = dot(xs_high[...], spread) + dot(xs_low[...], spread)
        wide = lambda ref: jnp.concatenate([ref[...]] * (CHUNK // 128), axis=1)
        fresh = wide(dec) * old[t] + values * wide(write)
        new[t] = fresh
        store_state(t).start()
        high, low = split(fresh * wide(read))
        y[...] += dot_nt(high, spread) + dot_nt(low, spread)
        return carry

    lax.fori_loop(0, CHUNKS, chunk_step, 0)

    loads[2].wait()
    gate = silu(dot(normed, gate_w[...]).astype(BF16).astype(F32))
    pieces = []
    for j in range(HEADS // 2):
        even = y[pl.ds(2 * j, ROWS, stride=HEADS), :]
        odd = y[pl.ds(2 * j + 1, ROWS, stride=HEADS), :]
        gain = jnp.where(low_half, skip[2 * j], skip[2 * j + 1])
        cols = slice(128 * j, 128 * j + 128)
        pieces.append(
            (jnp.where(low_half, even, odd) + gain * conv[:, cols]) * gate[:, cols]
        )
    groups = [jnp.concatenate(pieces[2 * g : 2 * g + 2], axis=1) for g in range(2)]
    inner = jnp.concatenate([rms(g) for g in groups], axis=1) * inner_gain[...]
    loads[3].wait()
    partial[...] = dot(inner.astype(BF16), out_w[...]).astype(BF16)
    for t in range(CHUNKS):
        store_state(t).wait()


def run_mixer(
    stream,
    mixer_gain,
    step_t,
    bias,
    decay,
    skip,
    input_taps,
    map_taps,
    input_past,
    map_past,
    inner_gain,
    ids,
    weights,
    gate_proj,
    input_proj,
    state_maps,
    mixer_out,
    state,
):
    vmem = pl.BlockSpec(memory_space=VMEM)
    smem = pl.BlockSpec(memory_space=pltpu.SMEM)
    hbm = pl.BlockSpec(memory_space=ANY)
    lanes = lambda: VMEM((256, 128), F32)
    return pl.pallas_call(
        mixer_kernel,
        out_shape=(
            jax.ShapeDtypeStruct((256, 4096), F32),
            jax.ShapeDtypeStruct((ROWS, 2 * HALF), BF16),
            jax.ShapeDtypeStruct((16, 256), BF16),
        ),
        in_specs=[vmem] * 3 + [smem] * 3 + [vmem] * 7 + [hbm] * 5,
        out_specs=(hbm, vmem, vmem),
        scratch_shapes=[
            VMEM((2048, 512), BF16),
            VMEM((2048, 512), BF16),
            VMEM((2, 2048, 128), BF16),
            VMEM((512, 2048), BF16),
            VMEM((CHUNKS, 256, CHUNK), F32),
            VMEM((CHUNKS, 256, CHUNK), F32),
            lanes(),
            lanes(),
            lanes(),
            VMEM((256, 128), BF16),
            VMEM((256, 128), BF16),
            lanes(),
            lanes(),
            pltpu.SemaphoreType.DMA((4 + 2 * CHUNKS,)),
        ],
        compiler_params=pltpu.CompilerParams(vmem_limit_bytes=40 * 2**20),
        name="mixer",
    )(
        stream,
        mixer_gain,
        step_t,
        bias,
        decay,
        skip,
        input_taps,
        map_taps,
        input_past,
        map_past,
        inner_gain,
        ids,
        weights,
        gate_proj,
        input_proj,
        state_maps,
        mixer_out,
        state,
    )


def ffn_kernel(
    partial,
    stream,
    gain,
    meta,
    mix,
    eg_hbm,
    eu_hbm,
    ed_hbm,
    dg_hbm,
    du_hbm,
    dd_hbm,
    out,
    x0,
    x1,
    x2,
    y0,
    y1,
    y2,
    s0,
    s1,
    s2,
    ra0,
    ra1,
    ra2,
    rb0,
    rb1,
    rb2,
    rc0,
    rc1,
    rc2,
    other_partial,
    wide,
    mid,
    eg,
    eu,
    ed,
    ed_other,
    dgu,
    dgu_other,
    dd,
    dd_scaled,
    packed,
    slot_weight,
    act,
    act_other,
    left_side,
    result,
    local_sem,
    ag_send,
    ag_recv,
    dd_send,
    dd_recv,
    rs_send,
    rs_recv,
    mi_send,
    mi_recv,
):
    ep = lax.axis_index("ep")
    core = lax.axis_index("tp")
    coords = (ep // 16, (ep // 4) % 4, ep % 4)
    other = 1 - core
    own_cols = pl.multiple_of(core * HALF, HALF)
    other_cols = pl.multiple_of(other * HALF, HALF)
    expert = ep // 8
    mine = (x0, x1, x2)
    theirs = (y0, y1, y2)
    sums = (s0, s1, s2)
    arrivals = ((rc0, rc1, rc2), (rb0, rb1, rb2), (ra0, ra1, ra2))

    def neighbour(dim, shift):
        moved = list(coords)
        moved[dim] = lax.rem(coords[dim] + shift, 4)
        return (moved[0] * 16 + moved[1] * 4 + moved[2], core)

    partner = (ep, other)

    barrier = pltpu.get_barrier_semaphore()
    for dim in range(3):
        for shift in (1, 3):
            pl.semaphore_signal(
                barrier, inc=1, device_id=neighbour(dim, shift), device_id_type=MESH
            )
    pl.semaphore_signal(barrier, inc=1, device_id=partner, device_id_type=MESH)
    pl.semaphore_wait(barrier, 7)

    def to_partner(src, dst, n):
        return pltpu.make_async_remote_copy(
            src_ref=src,
            dst_ref=dst,
            send_sem=mi_send.at[n],
            recv_sem=mi_recv.at[n],
            device_id=partner,
            device_id_type=MESH,
        )

    swap_partial = to_partner(partial, other_partial, 0)
    swap_partial.start()
    loads = [
        pltpu.make_async_copy(eg_hbm, eg.at[pl.ds(0, HIDDEN)], local_sem.at[0]),
        pltpu.make_async_copy(eu_hbm, eu.at[pl.ds(0, HIDDEN)], local_sem.at[1]),
        pltpu.make_async_copy(
            ed_hbm.at[:, pl.ds(own_cols, HALF)], ed.at[pl.ds(0, HIDDEN)], local_sem.at[2]
        ),
        pltpu.make_async_copy(dg_hbm, dgu.at[pl.ds(0, DENSE)], local_sem.at[3]),
        pltpu.make_async_copy(du_hbm, dgu.at[pl.ds(128, DENSE)], local_sem.at[4]),
        pltpu.make_async_copy(dd_hbm, dd, local_sem.at[5]),
    ]
    for load in loads:
        load.start()

    swap_partial.wait()
    mixed = partial[...].astype(F32) + other_partial[...].astype(F32)
    hidden = stream[...].astype(F32) + mixed
    mid[...] = hidden
    wide[...] = (rms(hidden) * gain[...]).astype(BF16)
    here = coords
    for p in range(3):
        cols = pl.ds(pl.multiple_of(own_cols + STARTS[p], 128), WIDTHS[p])
        mine[p][here[0], here[1], here[2], 0:ROWS, :] = wide[:, cols]
    x2[here[0], here[1], here[2], ROWS : ROWS + 16, :] = meta[...]

    def view(buf, p, k, j, half, rows=None):
        index = [None, None, None]
        free = sorted(ORDERS[p][:k])
        for q in range(3):
            dim = ORDERS[p][q]
            if q < k:
                index[dim] = pl.ds(0, 4)
            elif q == k:
                index[dim] = j
            else:
                index[dim] = coords[dim]
        if half is not None:
            if free:
                index[free[0]] = pl.ds(2 * half, 2)
            else:
                index.append(pl.ds(16 * half, 16) if rows is None or half == 0 else rows)
        elif rows is not None:
            index.append(rows)
        return buf.at[tuple(index)]

    def turn(p, k, shift):
        return lax.rem(coords[ORDERS[p][k]] + shift, 4)

    def gather_copy(p, k, n, j, half, shift):
        rows = pl.ds(16, BLOCK_ROWS[p] - 16) if k == 0 else None
        where = view(mine[p], p, k, j, half, rows)
        at = 6 * (3 * k + p) + n
        return pltpu.make_async_remote_copy(
            src_ref=where,
            dst_ref=where,
            send_sem=ag_send.at[at],
            recv_sem=ag_recv.at[at],
            device_id=neighbour(ORDERS[p][k], shift),
            device_id_type=MESH,
        )

    hand_overs = []

    def hand_over(p, j, half, n):
        free = sorted(ORDERS[p][:2])
        rows = pl.ds(0, ROWS)

        def cut(buf):
            index = [None, None, None, rows]
            index[ORDERS[p][2]] = j
            for dim in free:
                index[dim] = pl.ds(0, 4)
            if half is not None:
                index[free[0]] = pl.ds(2 * half, 2)
            return buf.at[tuple(index)]

        copy = pltpu.make_async_remote_copy(
            src_ref=cut(mine[p]),
            dst_ref=cut(theirs[p]),
            send_sem=dd_send.at[7 * p + n],
            recv_sem=dd_recv.at[7 * p + n],
            device_id=partner,
            device_id_type=MESH,
        )
        copy.start()
        hand_overs.append(copy)

    for k in range(3):
        copies = []
        for p in range(3):
            me, right, left = turn(p, k, 0), turn(p, k, 1), turn(p, k, 3)
            table = [
                gather_copy(p, k, 0, me, 0, 1),
                gather_copy(p, k, 1, me, 1, 1),
                gather_copy(p, k, 2, me, 1, 3),
                gather_copy(p, k, 3, me, 0, 3),
                gather_copy(p, k, 4, left, 0, 1),
                gather_copy(p, k, 5, right, 1, 3),
            ]
            copies.append(table)
            table[0].start()
            table[2].start()
            table[1].start()
            table[3].start()
            if k == 2:
                hand_over(p, me, None, 0)
        if k == 0:
            early = [
                to_partner(
                    ed_hbm.at[:, pl.ds(other_cols, HALF)], ed_other.at[pl.ds(0, HIDDEN)], 1
                ),
                to_partner(dg_hbm, dgu_other.at[pl.ds(0, DENSE)], 2),
                to_partner(du_hbm, dgu_other.at[pl.ds(128, DENSE)], 3),
            ]
            for copy in early:
                copy.start()
            for ref in (eg, eu, ed, ed_other):
                ref[HIDDEN:HPAD, :] = jnp.zeros((HPAD - HIDDEN, ref.shape[1]), BF16)
            for ref in (dgu, dgu_other):
                ref[DENSE:128, :] = jnp.zeros((128 - DENSE, HALF), BF16)
                ref[128 + DENSE : 256, :] = jnp.zeros((128 - DENSE, HALF), BF16)
            dd_scaled[DENSE:128, :] = jnp.zeros((128 - DENSE, HALF), BF16)
            for g in range(GROUPS):
                result[g, SLOTS:128, :] = jnp.zeros((128 - SLOTS, HALF), BF16)
        for p in range(3):
            left, right = turn(p, k, 3), turn(p, k, 1)
            copies[p][0].wait_recv()
            copies[p][4].start()
            copies[p][2].wait_recv()
            copies[p][5].start()
            if k == 2:
                hand_over(p, left, 0, 1)
                hand_over(p, right, 1, 2)
        for p in range(3):
            left, right, far = turn(p, k, 3), turn(p, k, 1), turn(p, k, 2)
            copies[p][1].wait_recv()
            copies[p][3].wait_recv()
            if k == 2:
                hand_over(p, left, 1, 3)
                hand_over(p, right, 0, 4)
        for p in range(3):
            far = turn(p, k, 2)
            copies[p][4].wait_recv()
            copies[p][5].wait_recv()
            if k == 2:
                hand_over(p, far, 0, 5)
                hand_over(p, far, 1, 6)
        for p in range(3):
            for copy in copies[p]:
                copy.wait_send()
    for copy in hand_overs:
        copy.wait()
    for load in loads:
        load.wait()
    for copy in early:
        copy.wait()

    pick_row = lax.broadcasted_iota(jnp.int32, (128, 128), 0)
    pick_rank = (pick_row == expert).astype(F32).astype(BF16)
    pick_weight = (
        jnp.logical_or(pick_row == expert + 8, pick_row == expert + 16)
    ).astype(F32).astype(BF16)
    lane = lax.broadcasted_iota(jnp.int32, (GROUP_ROWS, 128), 1)
    source = lax.broadcasted_iota(jnp.int32, (GROUP_ROWS, 128), 0) // ROWS

    def group_of(bufs, g):
        z, y = g // 2, 2 * lax.rem(g, 2)
        return jnp.concatenate(
            [
                bufs[p][z, pl.ds(y, 2), :, 0:ROWS, :].reshape(GROUP_ROWS, WIDTHS[p])
                for p in range(3)
            ],
            axis=1,
        )

    def pack_group(g, carry):
        z, y = g // 2, 2 * lax.rem(g, 2)
        tags = x2[z, pl.ds(y, 2), :, ROWS : ROWS + 16, :].reshape(8, 16, 256)
        tags = jnp.concatenate([tags[:, :, 0:128], tags[:, :, 128:256]], axis=1)
        tags = tags.reshape(GROUP_ROWS, 128)
        rank = dot(tags, pick_rank).astype(jnp.int32)
        hit = jnp.logical_and(rank > 0, rank + (CAP * source - 1) == lane)
        table = hit.astype(F32).astype(BF16)
        left_side[g, :, 0:128] = table
        used = table[:, 0:SLOTS]
        slots = pl.ds(pl.multiple_of(g * SLOTS, SLOTS), SLOTS)
        packed[slots, pl.ds(own_cols, HALF)] = dot_tn(used, group_of(mine, g)).astype(BF16)
        packed[slots, pl.ds(other_cols, HALF)] = dot_tn(used, group_of(theirs, g)).astype(
            BF16
        )
        slot_tags = dot_tn(used, tags).astype(BF16)
        slot_weight[slots, :] = dot(slot_tags, pick_weight)
        return carry

    lax.fori_loop(0, GROUPS, pack_group, 0)

    sends = []
    for i in range(2):
        rows = pl.ds(i * 384, 384)
        taken = packed[rows, :]
        gate = dot_nt(taken, eg[...])
        up = dot_nt(taken, eu[...])
        act[rows, :] = (silu(gate) * up * slot_weight[rows, 0:1]).astype(BF16)
        copy = to_partner(act.at[rows], act_other.at[rows], 4 + i)
        copy.start()
        sends.append(copy)

    def dense_group(g, carry):
        both = dot_nt(group_of(mine, g), dgu[...]) + dot_nt(group_of(theirs, g), dgu_other[...])
        left_side[g, :, 128:256] = (silu(both[:, 0:128]) * both[:, 128:256]).astype(BF16)
        return carry

    lax.fori_loop(0, GROUPS, dense_group, 0)
    share = 1.0 / (1.0 + jnp.exp(-mix[...]))
    dd_scaled[0:DENSE, :] = (dd[...].astype(F32) * share).astype(BF16)

    for i in range(2):
        rows = pl.ds(i * 384, 384)
        sends[i].wait()
        back = dot(act[rows, :], ed[...]) + dot(act_other[rows, :], ed_other[...])
        result[pl.ds(4 * i, 4), 0:SLOTS, :] = back.astype(BF16).reshape(4, SLOTS, HALF)

    def spread_group(g, carry):
        z, y = g // 2, 2 * lax.rem(g, 2)
        total = dot(left_side[g], jnp.concatenate([result[g], dd_scaled[...]], axis=0))
        for p in range(3):
            cut = total[:, STARTS[p] : STARTS[p] + WIDTHS[p]].astype(BF16)
            sums[p][z, pl.ds(y, 2)] = cut.reshape(2, 4, ROWS, WIDTHS[p])
        return carry

    lax.fori_loop(0, GROUPS, spread_group, 0)

    def scatter_copy(p, k, n, j, half, shift):
        at = 6 * (3 * k + p) + n
        return pltpu.make_async_remote_copy(
            src_ref=view(sums[p], p, k, j, half),
            dst_ref=arrivals[k][p].at[n],
            send_sem=rs_send.at[at],
            recv_sem=rs_recv.at[at],
            device_id=neighbour(ORDERS[p][k], shift),
            device_id_type=MESH,
        )

    def add_in(p, k, j, half, slots):
        got = arrivals[k][p]
        if k == 0:
            rows = pl.ds(16 * half, 16)
            ref = sums[p].at[
                tuple(j if d == ORDERS[p][0] else coords[d] for d in range(3)) + (rows,)
            ]
            total = ref[...].astype(F32)
            for n in slots:
                total = total + got[n].astype(F32)
            ref[...] = total.astype(BF16)
            return
        free = sorted(ORDERS[p][:k])

        def block(t, carry):
            place = [coords[0], coords[1], coords[2]]
            place[ORDERS[p][k]] = j
            if k == 2:
                a, b = t // 4, lax.rem(t, 4)
                place[free[0]], place[free[1]] = 2 * half + a, b
                inner = (a, b)
            else:
                place[free[0]] = 2 * half + t
                inner = (t,)
            place = tuple(place)
            total = sums[p][place].astype(F32)
            for n in slots:
                total = total + got[(n,) + inner].astype(F32)
            sums[p][place] = total.astype(BF16)
            return carry

        lax.fori_loop(0, 8 if k == 2 else 2, block, 0)

    for k in (2, 1, 0):
        copies = []
        for p in range(3):
            right, far, left = turn(p, k, 1), turn(p, k, 2), turn(p, k, 3)
            table = [
                scatter_copy(p, k, 0, far, 0, 1),
                scatter_copy(p, k, 1, right, 1, 1),
                scatter_copy(p, k, 2, far, 1, 3),
                scatter_copy(p, k, 3, left, 0, 3),
                scatter_copy(p, k, 4, right, 0, 1),
                scatter_copy(p, k, 5, left, 1, 3),
            ]
            copies.append(table)
            table[0].start()
            table[2].start()
            table[1].start()
            table[3].start()
        for p in range(3):
            copies[p][0].wait_recv()
            add_in(p, k, turn(p, k, 1), 0, (0,))
            copies[p][4].start()
            copies[p][2].wait_recv()
            add_in(p, k, turn(p, k, 3), 1, (2,))
            copies[p][5].start()
        for p in range(3):
            copies[p][3].wait_recv()
            copies[p][4].wait_recv()
            if k > 0:
                add_in(p, k, turn(p, k, 0), 0, (3, 4))
            copies[p][1].wait_recv()
            copies[p][5].wait_recv()
            if k > 0:
                add_in(p, k, turn(p, k, 0), 1, (1, 5))
        for p in range(3):
            for copy in copies[p]:
                copy.wait_send()

    for p in range(3):
        got = arrivals[0][p]
        for half, slots in ((0, (3, 4)), (1, (1, 5))):
            rows = pl.ds(16 * half, 16)
            total = sums[p][here[0], here[1], here[2], rows, :].astype(F32)
            for n in slots:
                total = total + got[n].astype(F32)
            cols = pl.ds(pl.multiple_of(own_cols + STARTS[p], 128), WIDTHS[p])
            kept = mid[rows, cols]
            out[rows, STARTS[p] : STARTS[p] + WIDTHS[p]] = (kept + total).astype(BF16)


def run_ffn(partial, stream, gain, meta, mix, eg, eu, ed, dg, du, dd):
    vmem = pl.BlockSpec(memory_space=VMEM)
    hbm = pl.BlockSpec(memory_space=ANY)
    blocks = lambda *lead: [VMEM((*lead, WIDTHS[p]), BF16) for p in range(3)]
    sem = pltpu.SemaphoreType.DMA
    return pl.pallas_call(
        ffn_kernel,
        out_shape=jax.ShapeDtypeStruct((ROWS, HALF), BF16),
        in_specs=[vmem] * 5 + [hbm] * 6,
        out_specs=vmem,
        scratch_shapes=[
            *[VMEM((4, 4, 4, BLOCK_ROWS[p], WIDTHS[p]), BF16) for p in range(3)],
            *blocks(4, 4, 4, ROWS),
            *blocks(4, 4, 4, ROWS),
            *blocks(6, 2, 4, ROWS),
            *blocks(6, 2, ROWS),
            *blocks(6, 16),
            VMEM((ROWS, 2 * HALF), BF16),
            VMEM((ROWS, 2 * HALF), BF16),
            VMEM((ROWS, 2 * HALF), F32),
            VMEM((HPAD, 2 * HALF), BF16),
            VMEM((HPAD, 2 * HALF), BF16),
            VMEM((HPAD, HALF), BF16),
            VMEM((HPAD, HALF), BF16),
            VMEM((256, HALF), BF16),
            VMEM((256, HALF), BF16),
            VMEM((DENSE, HALF), BF16),
            VMEM((128, HALF), BF16),
            VMEM((GROUPS * SLOTS, 2 * HALF), BF16),
            VMEM((GROUPS * SLOTS, 128), F32),
            VMEM((GROUPS * SLOTS, HPAD), BF16),
            VMEM((GROUPS * SLOTS, HPAD), BF16),
            VMEM((GROUPS, GROUP_ROWS, 256), BF16),
            VMEM((GROUPS, 128, HALF), BF16),
            sem((6,)),
            sem((54,)),
            sem((54,)),
            sem((21,)),
            sem((21,)),
            sem((54,)),
            sem((54,)),
            sem((6,)),
            sem((6,)),
        ],
        compiler_params=pltpu.CompilerParams(
            collective_id=0, has_side_effects=True, vmem_limit_bytes=60 * 2**20
        ),
        name="ffn",
    )(partial, stream, gain, meta, mix, eg, eu, ed, dg, du, dd)


def local(
    stream,
    mixer_gain,
    gate_proj,
    input_proj,
    state_maps,
    step_proj,
    step_bias,
    decay_rate,
    input_taps,
    map_taps,
    input_past,
    map_past,
    head_state,
    skip_gain,
    inner_gain,
    mixer_out,
    channel_gain,
    expert_ids,
    expert_weight,
    expert_gate,
    expert_up,
    expert_down,
    dense_gate,
    dense_up,
    dense_down,
    dense_mix,
):
    state_out, partial, meta = run_mixer(
        stream,
        mixer_gain.reshape(1, -1),
        step_proj.T,
        step_bias,
        decay_rate,
        skip_gain,
        input_taps,
        map_taps,
        jnp.transpose(input_past, (1, 0, 2)),
        jnp.transpose(map_past, (1, 2, 0, 3)).reshape(6, ROWS, 128),
        inner_gain.reshape(1, -1),
        expert_ids.T,
        expert_weight.T,
        gate_proj,
        input_proj,
        state_maps,
        mixer_out,
        head_state.reshape(256, 4096),
    )
    out = run_ffn(
        partial,
        stream,
        channel_gain.reshape(1, -1),
        meta,
        dense_mix.reshape(1, -1),
        expert_gate.T,
        expert_up.T,
        expert_down,
        dense_gate.T,
        dense_up.T,
        dense_down,
    )
    return out, state_out.reshape(head_state.shape)


def solution(mesh):
    placed = (
        P("ep", None),
        P(),
        P(None, "tp"),
        P(None, "tp"),
        P(None, None, "tp"),
        P(None, "tp"),
        P("tp"),
        P("tp"),
        P(None, "tp"),
        P(None, None, "tp"),
        P("ep", None, "tp"),
        P("ep", None, None, "tp"),
        P("ep", "tp", None),
        P("tp"),
        P("tp"),
        P("tp", None),
        P(),
        P("ep", None),
        P("ep", None),
        P(None, ("ep", "tp")),
        P(None, ("ep", "tp")),
        P(("ep", "tp"), None),
        P("tp", "ep"),
        P("tp", "ep"),
        P("ep", "tp"),
        P("tp"),
    )
    return jax.shard_map(
        local,
        mesh=mesh,
        in_specs=placed,
        out_specs=(P("ep", "tp"), P("ep", "tp", None)),
        check_vma=False,
    )
```

time: 428 us -> 119 us (0.28)
  blocking collectives: 226 us -> 0 us
  Pallas kernels: 0 us -> 97 us
  waiting for transfers between devices: 41.7 us -> 0 us
  matrix products: 40.7 us -> 0 us
  other arithmetic: 40.6 us -> 0 us
  local copies, waits for them, and re-layouts: 42.3 us -> 20.3 us
  starting transfers between devices: 21.3 us -> 0 us
  between operations: 14.7 us -> 0.68 us
    all_gather x1 -> x0, blocking collectives: 215 us -> none  [side_by_side(): out = lax.all_gather(both, axis, axis=dim, tiled=True)]
    pallas_call x0 -> x2, Pallas kernels: none -> 97 us  [the longest x1 88.7 us: run_ffn(): pl.pallas_call(ffn_kernel, out_shape=jax.ShapeDtypeStruct((ROWS, HALF), B...]
    all_to_all x3 -> x0, waiting for transfers between devices: 41.7 us -> none  [the longest x1 40.2 us: summed_on_arrival(): lax.all_to_all(in_blocks(array, dim, devices), axis, 0, 0, tiled=True)]
    dot_general x13 -> x0, matrix products: 40.7 us -> none  [the longest x1 10.2 us: local(): jnp.einsum('bsc,bcd->bsd', combine, halves, precision=lax.Precision.HIGHEST)]
    all_to_all x3 -> x0, starting transfers between devices: 21.3 us -> none  [the longest x1 11.9 us: local(): lax.all_to_all(outgoing, 'ep', split_axis=0, concat_axis=0, tiled=True)]
    unnamed x38 -> x39, local copies, waits for them, and re-layouts: 0.99 us -> 19.5 us
    another operation x3 -> x0, other arithmetic: 15.5 us -> none  [the longest x1 15.4 us: local(): source_rank = jnp.cumsum(matched, axis=1) - 1]
    reshape x3 -> x0, local copies, waits for them, and re-layouts: 14.1 us -> none  [the longest x1 7.87 us: mix_heads(): state_old = head_state.reshape(row_count, head_count, HEAD, NSTATE)]
  transfers between devices with their start and end apart: 4 -> 0, of which waited for: 2 -> 0; matrix products, arithmetic and copies ran while one was open for 18% -> 0% of each run, Pallas kernels for 0% -> 0%
where the time goes in v1:
time: 119 us; the launch traced here: 118 us
  Pallas kernels  97 us (82%)
  local copies, waits for them, and re-layouts  20.3 us (17%)
    pallas_call x1, Pallas kernels, run_ffn(): pl.pallas_call(ffn_kernel, out_shape=jax.ShapeDtypeStruct((ROWS, HALF), B...  88.7 us
    unnamed x39, local copies, waits for them, and re-layouts  19.5 us
    pallas_call x1, Pallas kernels, run_mixer(): pl.pallas_call(mixer_kernel, out_shape=(jax.ShapeDtypeStruct((256, 4096),...  8.32 us

profile of v1, /device:TPU:0, one launch (start us, length us, event | category | flops | bytes accessed | tf_op | source)
XLA Modules:
  0.0 118.0 jit_solution(945590731532187111)
XLA Ops:
  0.6 0.8 copy.28
  1.4 0.0 copy-start
  1.4 2.2 %copy-done = f32[32,8,4096]{2,1,0:T(8,128)S(1)} copy-done((f32[32,8,4096]{2,1,0:T(8,128)S(1)}, f32[32,8,4096]{2,1,0:T(8,128)}, u32[]{:S(2)}) %copy-start) | copy-done | bytes 4194328
  3.6 0.0 copy-start.1
  3.6 1.6 %copy-done.1 = bf16[2048,512]{1,0:T(8,128)(2,1)S(1)} copy-done((bf16[2048,512]{1,0:T(8,128)(2,1)S(1)}, bf16[2048,512]{1,0:T(8,128)(2,1)}, u32[]{:S(2)}) %copy-start.1) | copy-done | bytes 2097176
  5.2 0.0 copy-start.2
  5.2 1.6 %copy-done.2 = bf16[2048,512]{1,0:T(8,128)(2,1)S(1)} copy-done((bf16[2048,512]{1,0:T(8,128)(2,1)S(1)}, bf16[2048,512]{1,0:T(8,128)(2,1)}, u32[]{:S(2)}) %copy-start.2) | copy-done | bytes 2097176
  6.8 0.0 copy-start.3
  6.8 1.6 %copy-done.3 = bf16[512,2048]{1,0:T(8,128)(2,1)S(1)} copy-done((bf16[512,2048]{1,0:T(8,128)(2,1)S(1)}, bf16[512,2048]{1,0:T(8,128)(2,1)}, u32[]{:S(2)}) %copy-start.3) | copy-done | bytes 2097176
  8.4 0.0 copy-start.4
  8.4 1.2 %copy-done.4 = bf16[2,2048,128]{2,1,0:T(8,128)(2,1)S(1)} copy-done((bf16[2,2048,128]{2,1,0:T(8,128)(2,1)S(1)}, bf16[2,2048,128]{2,1,0:T(8,128)(2,1)}, u32[]{:S(2)}) %copy-start.4) | copy-done | bytes 1048600
  9.6 0.0 copy-start.5
  9.6 0.9 copy-done.5
  10.5 0.0 copy-start.7
  10.5 0.9 copy-done.7
  11.4 0.8 copy-done.8
  12.2 0.0 copy-start.10
  12.2 0.7 copy-done.10
  12.9 0.7 copy-done.11
  13.6 0.7 copy-done.12
  14.3 0.7 copy-done.13
  14.9 0.7 copy-done.14
  15.6 0.7 copy-done.15
  16.3 0.7 copy-done.16
  17.0 0.7 copy-done.17
  17.6 0.7 copy-done.18
  18.3 8.3 %mixer.1 = (f32[256,4096]{1,0:T(8,128)}, bf16[32,2048]{1,0:T(8,128)(2,1)S(1)}, bf16[16,256]{1,0:T(8,128)(2,1)S(1)}) custom-call(bf16[32,2048]{1,0:T(8,128)(2,1)S(1)} %copy-done.5, f32[1,2048]{1,0:T(1,128)S(1)} %bitcast.20, bf16[8,2048]{1,0:T(8,128)(2,1)S(1)} %bitcast.19, f32[8]{0:T(128)S(1)} %copy-done.16, f32[8]{0:T(128)S(1)} %copy-done.17, ...), custom_call_target="tpu_custom_call" | custom-call | tf_op jit(solution)/shard_map/mixer/pallas_call | solution.py:248
  26.6 0.0 copy-start.6
  26.6 0.6 copy-done.6
  27.3 0.6 copy-done.9
  27.9 88.7 %ffn.1 = bf16[32,1024]{1,0:T(8,128)(2,1)} custom-call(bf16[32,2048]{1,0:T(8,128)(2,1)} %copy-done.6, bf16[32,2048]{1,0:T(8,128)(2,1)} %stream.3, f32[1,2048]{1,0:T(1,128)} %bitcast.29, bf16[16,256]{1,0:T(8,128)(2,1)} %copy-done.9, f32[1,1024]{1,0:T(1,128)} %bitcast.30, bf16[448,2048]{1,0:T(8,128)(2,1)} %bitcast.24, bf16[448,2048]{1,0:T(8,128)(2,1)} %bitcast.25, ...), custom_call_target="tpu_custom_call" | custom-call | tf_op jit(solution)/shard_map/ffn/pallas_call | solution.py:724
  116.6 1.5 %copy.30 = bf16[32,1024]{1,0:T(8,128)(2,1)} copy(bf16[32,1024]{1,0:T(8,128)(2,1)} %ffn.1) | data formatting | bytes 131072
  (10 shorter events, 0.0 us)
Async XLA Ops:
  1.4 2.2 %copy-start = (f32[32,8,4096]{2,1,0:T(8,128)S(1)}, f32[32,8,4096]{2,1,0:T(8,128)}, u32[]{:S(2)}) copy-start(f32[32,8,4096]{2,1,0:T(8,128)} %param.38) | copy-start | bytes 12582916
  3.6 1.6 %copy-start.1 = (bf16[2048,512]{1,0:T(8,128)(2,1)S(1)}, bf16[2048,512]{1,0:T(8,128)(2,1)}, u32[]{:S(2)}) copy-start(bf16[2048,512]{1,0:T(8,128)(2,1)} %gate_hbm.1) | copy-start | bytes 6291460
  5.2 1.6 %copy-start.2 = (bf16[2048,512]{1,0:T(8,128)(2,1)S(1)}, bf16[2048,512]{1,0:T(8,128)(2,1)}, u32[]{:S(2)}) copy-start(bf16[2048,512]{1,0:T(8,128)(2,1)} %input_hbm.1) | copy-start | bytes 6291460
  6.8 1.6 %copy-start.3 = (bf16[512,2048]{1,0:T(8,128)(2,1)S(1)}, bf16[512,2048]{1,0:T(8,128)(2,1)}, u32[]{:S(2)}) copy-start(bf16[512,2048]{1,0:T(8,128)(2,1)} %out_hbm.1) | copy-start | bytes 6291460
  8.4 1.2 %copy-start.4 = (bf16[2,2048,128]{2,1,0:T(8,128)(2,1)S(1)}, bf16[2,2048,128]{2,1,0:T(8,128)(2,1)}, u32[]{:S(2)}) copy-start(bf16[2,2048,128]{2,1,0:T(8,128)(2,1)} %maps_hbm.1) | copy-start | bytes 3145732
  9.6 0.9 copy-start.5
  10.5 0.9 copy-start.7
  11.4 0.8 copy-start.8
  12.2 0.7 copy-start.10
  12.9 0.7 copy-start.11
  13.6 0.7 copy-start.12
  14.3 0.7 copy-start.13
  14.9 0.7 copy-start.14
  15.6 0.7 copy-start.15
  16.3 0.7 copy-start.16
  17.0 0.7 copy-start.17
  17.6 0.7 copy-start.18
  26.6 0.7 copy-start.6
  27.3 0.6 copy-start.9

commit v2 on v1

v2 whole, which is shorter than its diff:
```python
import functools

import jax
import jax.numpy as jnp
from jax import lax
from jax.experimental import pallas as pl
from jax.experimental.pallas import tpu as pltpu
from jax.sharding import PartitionSpec as P

EPS = 1e-06
MESH = pl.DeviceIdType.MESH
F32 = jnp.float32
BF16 = jnp.bfloat16
VMEM = pltpu.VMEM
ANY = pl.ANY

HEADS = 8
ROWS = 32
EXPERTS = 8
CAP = 12
CHUNKS = 8
CHUNK = 512
GROUPS = 8
GROUP_ROWS = 256
SLOTS = 96
HALF = 1024
HIDDEN = 448
HPAD = 512
DENSE = 88

WIDTHS = (384, 384, 256)
STARTS = (0, 384, 768)
BLOCK_ROWS = (32, 32, 48)
ORDERS = ((2, 1, 0), (1, 0, 2), (0, 2, 1))


def dot(a, b):
    return jnp.dot(a, b, preferred_element_type=F32)


def dot_nt(a, b):
    return lax.dot_general(a, b, (((1,), (1,)), ((), ())), preferred_element_type=F32)


def dot_tn(a, b):
    return lax.dot_general(a, b, (((0,), (0,)), ((), ())), preferred_element_type=F32)


def silu(v):
    return v / (1.0 + jnp.exp(-v))


def rms(v):
    return v * lax.rsqrt(jnp.mean(v * v, axis=-1, keepdims=True) + EPS)


def split(v):
    high = v.astype(BF16)
    return high, (v - high.astype(F32)).astype(BF16)


def mixer_kernel(*refs):
    given, refs = refs[:18], refs[18:]
    state_hbm = given[17]
    state_out, partial, meta = refs[:3]
    held, refs = refs[3:20], refs[20:]
    (
        stream,
        mixer_gain,
        step_t,
        ids,
        weights,
        bias,
        decay,
        skip,
        input_w,
        input_taps,
        input_past,
        maps_w,
        map_taps,
        map_past,
        inner_gain,
        gate_w,
        out_w,
    ) = held
    old, new, dec, write, read, xs_high, xs_low, tmp, y, past, in_sems, sems = refs
    loads = [
        pltpu.make_async_copy(src, dst, in_sems.at[n])
        for n, (src, dst) in enumerate(zip(given, held))
    ]

    def load_state(t):
        cols = pl.ds(pl.multiple_of(t * CHUNK, CHUNK), CHUNK)
        return pltpu.make_async_copy(state_hbm.at[:, cols], old.at[t], sems.at[t])

    def store_state(t):
        cols = pl.ds(pl.multiple_of(t * CHUNK, CHUNK), CHUNK)
        return pltpu.make_async_copy(
            new.at[t], state_out.at[:, cols], sems.at[CHUNKS + t]
        )

    for load in loads[:15]:
        load.start()
    for t in range(CHUNKS):
        load_state(t).start()
    loads[15].start()
    loads[16].start()

    for load in loads[:8]:
        load.wait()
    normed = (rms(stream[...].astype(F32)) * mixer_gain[...]).astype(BF16)
    steps = dot_nt(normed, step_t[...])

    expert_of = lax.broadcasted_iota(jnp.int32, (EXPERTS, ROWS), 0)
    hit0 = (ids[0:1, :] == expert_of).astype(F32)
    hit1 = (ids[1:2, :] == expert_of).astype(F32)
    member = hit0 + hit1
    upper = (
        lax.broadcasted_iota(jnp.int32, (ROWS, ROWS), 0)
        <= lax.broadcasted_iota(jnp.int32, (ROWS, ROWS), 1)
    ).astype(BF16)
    rank = dot(member.astype(BF16), upper) * member
    weight = hit0 * weights[0:1, :] + hit1 * weights[1:2, :]
    w_high = weight.astype(BF16).astype(F32)
    w_low = weight - w_high
    table = jnp.concatenate(
        [rank, w_high, w_low, jnp.zeros((104, ROWS), F32)], axis=0
    ).astype(BF16)
    eye = (
        lax.broadcasted_iota(jnp.int32, (ROWS, ROWS), 0)
        == lax.broadcasted_iota(jnp.int32, (ROWS, ROWS), 1)
    ).astype(BF16)
    by_row = dot_nt(eye, table)
    meta[...] = jnp.concatenate([by_row[0:16], by_row[16:32]], axis=1).astype(BF16)

    for load in loads[8:11]:
        load.wait()
    newest = dot(normed, input_w[...]).astype(BF16).astype(F32)
    conv = newest * input_taps[3:4, :]
    for t in range(3):
        conv = conv + input_past[t].astype(F32) * input_taps[t : t + 1, :]
    conv = silu(conv)

    for load in loads[11:14]:
        load.wait()
    past[...] = map_past[...].astype(F32)
    conv_maps = []
    for m in range(2):
        new_map = dot(normed, maps_w[m]).astype(BF16).astype(F32)
        acc = new_map * map_taps[m, 3:4, :]
        for t in range(3):
            acc = acc + past[pl.ds(2 * t + m, ROWS, stride=6), :] * map_taps[m, t : t + 1, :]
        conv_maps.append(silu(acc))

    lane = lax.broadcasted_iota(jnp.int32, (ROWS, 128), 1)
    low_half = lane < 64

    def both_halves(v):
        turned = pltpu.roll(v, 64, 1)
        return jnp.where(low_half, v, turned), jnp.where(low_half, turned, v)

    write_by_group = both_halves(conv_maps[0])
    read_by_group = both_halves(conv_maps[1])
    for h in range(HEADS):
        rows = pl.ds(h, ROWS, stride=HEADS)
        v = jnp.broadcast_to(steps[:, h : h + 1], (ROWS, 128)) + bias[h]
        step = jnp.maximum(v, 0.0) + jnp.log1p(jnp.exp(-jnp.abs(v)))
        dec[rows, :] = jnp.exp(-decay[h] * step)
        pair = conv[:, 128 * (h // 2) : 128 * (h // 2) + 128]
        mine = low_half if h % 2 == 0 else jnp.logical_not(low_half)
        tmp[rows, :] = jnp.where(mine, step * pair, 0.0)
        write[rows, :] = write_by_group[h // 4]
        read[rows, :] = read_by_group[h // 4]
    high, low = split(tmp[...])
    xs_high[...] = high
    xs_low[...] = low
    y[...] = jnp.zeros_like(y)

    slot = lax.broadcasted_iota(jnp.int32, (128, CHUNK), 0) % 64
    place = lax.broadcasted_iota(jnp.int32, (128, CHUNK), 1) // 64

    def chunk_step(t, carry):
        spread = (slot == place + 8 * t).astype(F32).astype(BF16)
        load_state(t).wait()
        values = dot(xs_high[...], spread) + dot(xs_low[...], spread)
        wide = lambda ref: jnp.concatenate([ref[...]] * (CHUNK // 128), axis=1)
        fresh = wide(dec) * old[t] + values * wide(write)
        new[t] = fresh
        store_state(t).start()
        high, low = split(fresh * wide(read))
        y[...] += dot_nt(high, spread) + dot_nt(low, spread)
        return carry

    lax.fori_loop(0, CHUNKS, chunk_step, 0)

    loads[14].wait()
    loads[15].wait()
    gate = silu(dot(normed, gate_w[...]).astype(BF16).astype(F32))
    pieces = []
    for j in range(HEADS // 2):
        even = y[pl.ds(2 * j, ROWS, stride=HEADS), :]
        odd = y[pl.ds(2 * j + 1, ROWS, stride=HEADS), :]
        gain = jnp.where(low_half, skip[2 * j], skip[2 * j + 1])
        cols = slice(128 * j, 128 * j + 128)
        pieces.append(
            (jnp.where(low_half, even, odd) + gain * conv[:, cols]) * gate[:, cols]
        )
    groups = [jnp.concatenate(pieces[2 * g : 2 * g + 2], axis=1) for g in range(2)]
    inner = jnp.concatenate([rms(g) for g in groups], axis=1) * inner_gain[...]
    loads[16].wait()
    partial[...] = dot(inner.astype(BF16), out_w[...]).astype(BF16)
    for t in range(CHUNKS):
        store_state(t).wait()


def run_mixer(*given):
    vmem = pl.BlockSpec(memory_space=VMEM)
    hbm = pl.BlockSpec(memory_space=pltpu.HBM)
    lanes = lambda: VMEM((256, 128), F32)
    held = [
        (pltpu.SMEM if 5 <= n < 8 else VMEM)(v.shape, v.dtype)
        for n, v in enumerate(given[:17])
    ]
    return pl.pallas_call(
        mixer_kernel,
        out_shape=(
            jax.ShapeDtypeStruct((256, 4096), F32),
            jax.ShapeDtypeStruct((ROWS, 2 * HALF), BF16),
            jax.ShapeDtypeStruct((16, 256), BF16),
        ),
        in_specs=[hbm] * 18,
        out_specs=(hbm, vmem, vmem),
        scratch_shapes=[
            *held,
            VMEM((CHUNKS, 256, CHUNK), F32),
            VMEM((CHUNKS, 256, CHUNK), F32),
            lanes(),
            lanes(),
            lanes(),
            VMEM((256, 128), BF16),
            VMEM((256, 128), BF16),
            lanes(),
            lanes(),
            VMEM((192, 128), F32),
            pltpu.SemaphoreType.DMA((17,)),
            pltpu.SemaphoreType.DMA((2 * CHUNKS,)),
        ],
        compiler_params=pltpu.CompilerParams(vmem_limit_bytes=67043328),
        name="mixer",
    )(*given)


def ffn_kernel(
    partial,
    meta,
    stream_hbm,
    gain_hbm,
    mix_hbm,
    eg_hbm,
    eu_hbm,
    ed_hbm,
    dg_hbm,
    du_hbm,
    dd_hbm,
    out,
    x0,
    x1,
    x2,
    y0,
    y1,
    y2,
    s0,
    s1,
    s2,
    *rest,
):
    landed, rest = rest[:18], rest[18:]
    landing = [(landed[6 * k : 6 * k + 3], landed[6 * k + 3 : 6 * k + 6]) for k in range(3)]
    (
    other_partial,
    wide,
    mid,
    eg,
    eu,
    ed,
    ed_other,
    dgu,
    dgu_other,
    dd,
    dd_scaled,
    packed,
    slot_weight,
    act,
    act_other,
    left_side,
    result,
    local_sem,
    ag_send,
    ag_recv,
    dd_send,
    dd_recv,
    rs_send,
    rs_recv,
    mi_send,
    mi_recv,
    stream,
    gain,
    mix,
    small_sem,
    ) = rest
    ep = lax.axis_index("ep")
    core = lax.axis_index("tp")
    coords = (ep // 16, (ep // 4) % 4, ep % 4)
    other = 1 - core
    own_cols = pl.multiple_of(core * HALF, HALF)
    other_cols = pl.multiple_of(other * HALF, HALF)
    expert = ep // 8
    mine = (x0, x1, x2)
    theirs = (y0, y1, y2)
    sums = (s0, s1, s2)

    def neighbour(dim, shift):
        moved = list(coords)
        moved[dim] = lax.rem(coords[dim] + shift, 4)
        return (moved[0] * 16 + moved[1] * 4 + moved[2], core)

    partner = (ep, other)

    small = [
        pltpu.make_async_copy(stream_hbm, stream, small_sem.at[0]),
        pltpu.make_async_copy(gain_hbm, gain, small_sem.at[1]),
        pltpu.make_async_copy(mix_hbm, mix, small_sem.at[2]),
    ]
    for load in small:
        load.start()
    barrier = pltpu.get_barrier_semaphore()
    for dim in range(3):
        for shift in (1, 3):
            pl.semaphore_signal(
                barrier, inc=1, device_id=neighbour(dim, shift), device_id_type=MESH
            )
    pl.semaphore_signal(barrier, inc=1, device_id=partner, device_id_type=MESH)
    pl.semaphore_wait(barrier, 7)

    def to_partner(src, dst, n):
        return pltpu.make_async_remote_copy(
            src_ref=src,
            dst_ref=dst,
            send_sem=mi_send.at[n],
            recv_sem=mi_recv.at[n],
            device_id=partner,
            device_id_type=MESH,
        )

    swap_partial = to_partner(partial, other_partial, 0)
    swap_partial.start()
    loads = [
        pltpu.make_async_copy(eg_hbm, eg.at[pl.ds(0, HIDDEN)], local_sem.at[0]),
        pltpu.make_async_copy(eu_hbm, eu.at[pl.ds(0, HIDDEN)], local_sem.at[1]),
        pltpu.make_async_copy(
            ed_hbm.at[:, pl.ds(own_cols, HALF)], ed.at[pl.ds(0, HIDDEN)], local_sem.at[2]
        ),
        pltpu.make_async_copy(dg_hbm, dgu.at[pl.ds(0, DENSE)], local_sem.at[3]),
        pltpu.make_async_copy(du_hbm, dgu.at[pl.ds(128, DENSE)], local_sem.at[4]),
        pltpu.make_async_copy(dd_hbm, dd, local_sem.at[5]),
    ]
    for load in loads:
        load.start()

    for load in small:
        load.wait()
    swap_partial.wait()
    mixed = partial[...].astype(F32) + other_partial[...].astype(F32)
    hidden = stream[...].astype(F32) + mixed
    mid[...] = hidden
    wide[...] = (rms(hidden) * gain[...]).astype(BF16)
    here = coords
    for p in range(3):
        cols = pl.ds(pl.multiple_of(own_cols + STARTS[p], 128), WIDTHS[p])
        mine[p][here[0], here[1], here[2], 0:ROWS, :] = wide[:, cols]
    x2[here[0], here[1], here[2], ROWS : ROWS + 16, :] = meta[...]

    def cut(buf, p, where, half=None, rows=None):
        index = [None, None, None]
        for q in range(3):
            index[ORDERS[p][q]] = pl.ds(0, 4) if where[q] is None else where[q]
        if half is not None:
            free = sorted(ORDERS[p][q] for q in range(3) if where[q] is None)
            if free:
                index[free[0]] = pl.ds(2 * half, 2)
            else:
                rows = pl.ds(0, 16) if half == 0 else pl.ds(16, rows - 16)
        elif rows is not None:
            rows = pl.ds(0, rows)
        if rows is not None and not (half is not None and free):
            index.append(rows)
        return buf.at[tuple(index)]

    def turn(p, k, shift):
        return lax.rem(coords[ORDERS[p][k]] + shift, 4)

    ME, RIGHT, FAR, LEFT = 0, 1, 2, 3
    spots = [[[turn(p, k, shift) for shift in range(4)] for k in range(3)] for p in range(3)]

    class Ring:
        def __init__(self, p, k, at, place):
            self.p, self.k, self.place = p, k, place
            self.copies = [
                self.copy(at, ME, None, 1),
                self.copy(at + 1, ME, None, 3),
                self.copy(at + 2, LEFT, 0, 1),
                self.copy(at + 3, RIGHT, 1, 3),
            ]

        def copy(self, at, shift, half, to):
            p = self.p
            where = list(self.place)
            where[self.k] = spots[p][self.k][shift]
            rows = BLOCK_ROWS[p] if half is not None else None
            ref = cut(mine[p], p, where, half, rows)
            return pltpu.make_async_remote_copy(
                src_ref=ref,
                dst_ref=ref,
                send_sem=ag_send.at[at],
                recv_sem=ag_recv.at[at],
                device_id=neighbour(ORDERS[p][self.k], to),
                device_id_type=MESH,
            )

        def start(self):
            self.copies[0].start()
            self.copies[1].start()

        def on(self):
            self.copies[0].wait_recv()
            self.copies[2].start()
            self.copies[1].wait_recv()
            self.copies[3].start()

        def end(self):
            self.copies[2].wait_recv()
            self.copies[3].wait_recv()

    first, second, blocks, lines = [], [], [], []
    for p in range(3):
        at = 48 * p
        own = [spots[p][k][ME] for k in range(3)]
        first.append(Ring(p, 0, at, own))
        second.append(
            [Ring(p, 1, at + 4 + 4 * u, [spots[p][0][u], None, own[2]]) for u in range(4)]
        )
        blocks.append(
            [Ring(p, 2, at + 20 + 4 * u, [spots[p][0][u], own[1], None]) for u in range(4)]
        )
        lines.append(
            [Ring(p, 2, at + 36 + 4 * (u - 1), [None, spots[p][1][u], None]) for u in (1, 2, 3)]
        )
    rings = [first] + second + blocks + lines
    hand_overs = []

    def hand_over(p, n, second_at, third_at):
        where = [None, second_at, third_at]
        copy = pltpu.make_async_remote_copy(
            src_ref=cut(mine[p], p, where, None, ROWS),
            dst_ref=cut(theirs[p], p, where, None, ROWS),
            send_sem=dd_send.at[13 * p + n],
            recv_sem=dd_recv.at[13 * p + n],
            device_id=partner,
            device_id_type=MESH,
        )
        copy.start()
        hand_overs.append(copy)

    parts = range(3)
    for p in parts:
        first[p].start()
    for p in parts:
        second[p][ME].start()
    for p in parts:
        blocks[p][ME].start()

    early = [
        to_partner(
            ed_hbm.at[:, pl.ds(other_cols, HALF)], ed_other.at[pl.ds(0, HIDDEN)], 1
        ),
        to_partner(dg_hbm, dgu_other.at[pl.ds(0, DENSE)], 2),
        to_partner(du_hbm, dgu_other.at[pl.ds(128, DENSE)], 3),
    ]
    for copy in early:
        copy.start()

    for p in parts:
        first[p].on()
        for u in (LEFT, RIGHT):
            second[p][u].start()
            blocks[p][u].start()
    for p in parts:
        second[p][ME].on()
    for p in parts:
        blocks[p][ME].on()
    for p in parts:
        first[p].end()
        second[p][FAR].start()
        blocks[p][FAR].start()
    for p in parts:
        second[p][LEFT].on()
        second[p][RIGHT].on()
    for p in parts:
        blocks[p][LEFT].on()
        blocks[p][RIGHT].on()
    for p in parts:
        second[p][FAR].on()
        lines[p][RIGHT - 1].start()
        lines[p][LEFT - 1].start()
    for ref in (eg, eu, ed, ed_other):
        ref[HIDDEN:HPAD, :] = jnp.zeros((HPAD - HIDDEN, ref.shape[1]), BF16)
    for ref in (dgu, dgu_other):
        ref[DENSE:128, :] = jnp.zeros((128 - DENSE, HALF), BF16)
        ref[128 + DENSE : 256, :] = jnp.zeros((128 - DENSE, HALF), BF16)
    dd_scaled[DENSE:128, :] = jnp.zeros((128 - DENSE, HALF), BF16)
    for g in range(GROUPS):
        result[g, SLOTS:128, :] = jnp.zeros((128 - SLOTS, HALF), BF16)
    for p in parts:
        for u in range(4):
            second[p][u].end()
        lines[p][FAR - 1].start()
        hand_over(p, 0, None, spots[p][2][ME])
    for p in parts:
        blocks[p][FAR].on()
        hand_over(p, 1, spots[p][1][ME], spots[p][2][LEFT])
        hand_over(p, 2, spots[p][1][ME], spots[p][2][RIGHT])
    for n, u in ((3, RIGHT), (6, LEFT), (9, FAR)):
        for p in parts:
            lines[p][u - 1].on()
            hand_over(p, n, spots[p][1][u], spots[p][2][LEFT])
            hand_over(p, n + 1, spots[p][1][u], spots[p][2][RIGHT])
        for p in parts:
            if u == RIGHT:
                for v in range(4):
                    blocks[p][v].end()
                hand_over(p, n + 2, spots[p][1][ME], spots[p][2][FAR])
            else:
                done = RIGHT if u == LEFT else LEFT
                lines[p][done - 1].end()
                hand_over(p, n + 2, spots[p][1][done], spots[p][2][FAR])
    for p in parts:
        lines[p][FAR - 1].end()
        hand_over(p, 12, spots[p][1][FAR], spots[p][2][FAR])
    for load in loads:
        load.wait()
    for copy in early:
        copy.wait()
    for group in rings:
        for ring in group:
            for copy in ring.copies:
                copy.wait_send()
    for copy in hand_overs:
        copy.wait()

    pick_row = lax.broadcasted_iota(jnp.int32, (128, 128), 0)
    pick_rank = (pick_row == expert).astype(F32).astype(BF16)
    pick_weight = (
        jnp.logical_or(pick_row == expert + 8, pick_row == expert + 16)
    ).astype(F32).astype(BF16)
    lane = lax.broadcasted_iota(jnp.int32, (GROUP_ROWS, 128), 1)
    source = lax.broadcasted_iota(jnp.int32, (GROUP_ROWS, 128), 0) // ROWS

    def group_of(bufs, g):
        z, y = g // 2, 2 * lax.rem(g, 2)
        return jnp.concatenate(
            [
                bufs[p][z, pl.ds(y, 2), :, 0:ROWS, :].reshape(GROUP_ROWS, WIDTHS[p])
                for p in range(3)
            ],
            axis=1,
        )

    def pack_group(g, carry):
        z, y = g // 2, 2 * lax.rem(g, 2)
        tags = x2[z, pl.ds(y, 2), :, ROWS : ROWS + 16, :].reshape(8, 16, 256)
        tags = jnp.concatenate([tags[:, :, 0:128], tags[:, :, 128:256]], axis=1)
        tags = tags.reshape(GROUP_ROWS, 128)
        rank = dot(tags, pick_rank).astype(jnp.int32)
        hit = jnp.logical_and(rank > 0, rank + (CAP * source - 1) == lane)
        table = hit.astype(F32).astype(BF16)
        left_side[g, :, 0:128] = table
        used = table[:, 0:SLOTS]
        slots = pl.ds(pl.multiple_of(g * SLOTS, SLOTS), SLOTS)
        packed[slots, pl.ds(own_cols, HALF)] = dot_tn(used, group_of(mine, g)).astype(BF16)
        packed[slots, pl.ds(other_cols, HALF)] = dot_tn(used, group_of(theirs, g)).astype(
            BF16
        )
        slot_tags = dot_tn(used, tags).astype(BF16)
        slot_weight[slots, :] = dot(slot_tags, pick_weight)
        return carry

    lax.fori_loop(0, GROUPS, pack_group, 0)

    sends = []
    for i in range(2):
        rows = pl.ds(i * 384, 384)
        taken = packed[rows, :]
        gate = dot_nt(taken, eg[...])
        up = dot_nt(taken, eu[...])
        act[rows, :] = (silu(gate) * up * slot_weight[rows, 0:1]).astype(BF16)
        copy = to_partner(act.at[rows], act_other.at[rows], 4 + i)
        copy.start()
        sends.append(copy)

    def dense_group(g, carry):
        both = dot_nt(group_of(mine, g), dgu[...]) + dot_nt(group_of(theirs, g), dgu_other[...])
        left_side[g, :, 128:256] = (silu(both[:, 0:128]) * both[:, 128:256]).astype(BF16)
        return carry

    lax.fori_loop(0, GROUPS, dense_group, 0)
    share = 1.0 / (1.0 + jnp.exp(-mix[...]))
    dd_scaled[0:DENSE, :] = (dd[...].astype(F32) * share).astype(BF16)

    for i in range(2):
        rows = pl.ds(i * 384, 384)
        sends[i].wait()
        back = dot(act[rows, :], ed[...]) + dot(act_other[rows, :], ed_other[...])
        result[pl.ds(4 * i, 4), 0:SLOTS, :] = back.astype(BF16).reshape(4, SLOTS, HALF)

    def spread_group(g, carry):
        z, y = g // 2, 2 * lax.rem(g, 2)
        total = dot(left_side[g], jnp.concatenate([result[g], dd_scaled[...]], axis=0))
        for p in range(3):
            cut = total[:, STARTS[p] : STARTS[p] + WIDTHS[p]].astype(BF16)
            sums[p][z, pl.ds(y, 2)] = cut.reshape(2, 4, ROWS, WIDTHS[p])
        return carry

    lax.fori_loop(0, GROUPS, spread_group, 0)

    class Back:
        def __init__(self, p, k, at, place, slot):
            self.p, self.k, self.place, self.slot = p, k, place, slot
            self.halves, self.wholes = landing[k][0][p], landing[k][1][p]
            self.copies = [
                self.copy(at, FAR, 0, 1, self.halves.at[slot, 0]),
                self.copy(at + 1, FAR, 1, 3, self.halves.at[slot, 1]),
                self.copy(at + 2, RIGHT, None, 1, self.wholes.at[slot, 0]),
                self.copy(at + 3, LEFT, None, 3, self.wholes.at[slot, 1]),
            ]

        def spot(self, shift):
            where = list(self.place)
            where[self.k] = spots[self.p][self.k][shift]
            return where

        def copy(self, at, shift, half, to, target):
            p = self.p
            rows = ROWS if half is not None else None
            return pltpu.make_async_remote_copy(
                src_ref=cut(sums[p], p, self.spot(shift), half, rows),
                dst_ref=target,
                send_sem=rs_send.at[at],
                recv_sem=rs_recv.at[at],
                device_id=neighbour(ORDERS[p][self.k], to),
                device_id_type=MESH,
            )

        def start(self):
            self.copies[0].start()
            self.copies[1].start()

        def add_half(self, shift, half):
            p, got = self.p, self.halves
            where = self.spot(shift)
            place = [None, None, None]
            for q in range(3):
                place[ORDERS[p][q]] = where[q]
            free = [d for d in range(3) if place[d] is None]
            if not free:
                rows = pl.ds(16 * half, 16)
                ref = sums[p].at[tuple(place) + (rows,)]
                ref[...] = ref[...] + got[self.slot, half]
                return
            for t in range(2):
                place[free[0]] = 2 * half + t
                ref = sums[p].at[tuple(place)]
                ref[...] = ref[...] + got[self.slot, half, t]

        def on(self):
            self.copies[0].wait_recv()
            self.add_half(RIGHT, 0)
            self.copies[2].start()
            self.copies[1].wait_recv()
            self.add_half(LEFT, 1)
            self.copies[3].start()

        def arrive(self):
            self.copies[2].wait_recv()
            self.copies[3].wait_recv()

        def end(self):
            p, got = self.p, self.wholes
            self.arrive()
            where = self.spot(ME)
            place = [None, None, None]
            for q in range(3):
                place[ORDERS[p][q]] = where[q]
            free = [d for d in range(3) if place[d] is None]
            for t in range(4):
                place[free[0]] = t
                ref = sums[p].at[tuple(place)]
                total = ref[...].astype(F32) + got[self.slot, 0, t].astype(F32)
                ref[...] = (total + got[self.slot, 1, t].astype(F32)).astype(BF16)

    third, middle, last = [], [], []
    for p in parts:
        at = 24 * p
        own = [spots[p][k][ME] for k in range(3)]
        third.append(
            [Back(p, 2, at + 4 * u, [None, spots[p][1][u], None], u) for u in range(4)]
        )
        middle.append(Back(p, 1, at + 16, [None, None, own[2]], 0))
        last.append(Back(p, 0, at + 20, own, 0))
    order = (FAR, LEFT, RIGHT, ME)
    for u in order:
        for p in parts:
            third[p][u].start()
    for u in order:
        for p in parts:
            third[p][u].on()
    for u in order:
        for p in parts:
            third[p][u].end()
            if u == FAR:
                middle[p].start()
        if u == RIGHT:
            for p in parts:
                middle[p].on()
    for p in parts:
        middle[p].end()
        last[p].start()
    for p in parts:
        last[p].on()
    for p in parts:
        last[p].arrive()
        got = last[p].wholes
        total = mid[:, pl.ds(pl.multiple_of(own_cols + STARTS[p], 128), WIDTHS[p])]
        total = total + sums[p][here[0], here[1], here[2]].astype(F32)
        total = total + got[0, 0].astype(F32) + got[0, 1].astype(F32)
        out[:, STARTS[p] : STARTS[p] + WIDTHS[p]] = total.astype(BF16)
    for group in third + [middle, last]:
        for back in group:
            for copy in back.copies:
                copy.wait_send()


def run_ffn(partial, meta, stream, gain, mix, eg, eu, ed, dg, du, dd):
    vmem = pl.BlockSpec(memory_space=VMEM)
    hbm = pl.BlockSpec(memory_space=pltpu.HBM)
    blocks = lambda *lead: [VMEM((*lead, WIDTHS[p]), BF16) for p in range(3)]
    sem = pltpu.SemaphoreType.DMA
    return pl.pallas_call(
        ffn_kernel,
        out_shape=jax.ShapeDtypeStruct((ROWS, HALF), BF16),
        in_specs=[vmem] * 2 + [hbm] * 9,
        out_specs=vmem,
        scratch_shapes=[
            *[VMEM((4, 4, 4, BLOCK_ROWS[p], WIDTHS[p]), BF16) for p in range(3)],
            *blocks(4, 4, 4, ROWS),
            *blocks(4, 4, 4, ROWS),
            *blocks(1, 2, 16),
            *blocks(1, 2, ROWS),
            *blocks(1, 2, 2, ROWS),
            *blocks(1, 2, 4, ROWS),
            *blocks(4, 2, 2, ROWS),
            *blocks(4, 2, 4, ROWS),
            VMEM((ROWS, 2 * HALF), BF16),
            VMEM((ROWS, 2 * HALF), BF16),
            VMEM((ROWS, 2 * HALF), F32),
            VMEM((HPAD, 2 * HALF), BF16),
            VMEM((HPAD, 2 * HALF), BF16),
            VMEM((HPAD, HALF), BF16),
            VMEM((HPAD, HALF), BF16),
            VMEM((256, HALF), BF16),
            VMEM((256, HALF), BF16),
            VMEM((DENSE, HALF), BF16),
            VMEM((128, HALF), BF16),
            VMEM((GROUPS * SLOTS, 2 * HALF), BF16),
            VMEM((GROUPS * SLOTS, 128), F32),
            VMEM((GROUPS * SLOTS, HPAD), BF16),
            VMEM((GROUPS * SLOTS, HPAD), BF16),
            VMEM((GROUPS, GROUP_ROWS, 256), BF16),
            VMEM((GROUPS, 128, HALF), BF16),
            sem((6,)),
            sem((144,)),
            sem((144,)),
            sem((39,)),
            sem((39,)),
            sem((72,)),
            sem((72,)),
            sem((6,)),
            sem((6,)),
            VMEM((ROWS, 2 * HALF), BF16),
            VMEM((1, 2 * HALF), F32),
            VMEM((1, HALF), F32),
            sem((3,)),
        ],
        compiler_params=pltpu.CompilerParams(
            collective_id=0, has_side_effects=True, vmem_limit_bytes=67043328
        ),
        name="ffn",
    )(partial, meta, stream, gain, mix, eg, eu, ed, dg, du, dd)


def local(
    stream,
    mixer_gain,
    gate_proj,
    input_proj,
    state_maps,
    step_proj,
    step_bias,
    decay_rate,
    input_taps,
    map_taps,
    input_past,
    map_past,
    head_state,
    skip_gain,
    inner_gain,
    mixer_out,
    channel_gain,
    expert_ids,
    expert_weight,
    expert_gate,
    expert_up,
    expert_down,
    dense_gate,
    dense_up,
    dense_down,
    dense_mix,
):
    state_out, partial, meta = run_mixer(
        stream,
        mixer_gain.reshape(1, -1),
        step_proj.T,
        expert_ids.T,
        expert_weight.T,
        step_bias,
        decay_rate,
        skip_gain,
        input_proj,
        input_taps,
        jnp.transpose(input_past, (1, 0, 2)),
        state_maps,
        map_taps,
        jnp.transpose(map_past, (0, 2, 1, 3)).reshape(192, 128),
        inner_gain.reshape(1, -1),
        gate_proj,
        mixer_out,
        head_state.reshape(256, 4096),
    )
    out = run_ffn(
        partial,
        meta,
        stream,
        channel_gain.reshape(1, -1),
        dense_mix.reshape(1, -1),
        expert_gate.T,
        expert_up.T,
        expert_down,
        dense_gate.T,
        dense_up.T,
        dense_down,
    )
    return out, state_out.reshape(head_state.shape)


def solution(mesh):
    placed = (
        P("ep", None),
        P(),
        P(None, "tp"),
        P(None, "tp"),
        P(None, None, "tp"),
        P(None, "tp"),
        P("tp"),
        P("tp"),
        P(None, "tp"),
        P(None, None, "tp"),
        P("ep", None, "tp"),
        P("ep", None, None, "tp"),
        P("ep", "tp", None),
        P("tp"),
        P("tp"),
        P("tp", None),
        P(),
        P("ep", None),
        P("ep", None),
        P(None, ("ep", "tp")),
        P(None, ("ep", "tp")),
        P(("ep", "tp"), None),
        P("tp", "ep"),
        P("tp", "ep"),
        P("ep", "tp"),
        P("tp"),
    )
    return jax.shard_map(
        local,
        mesh=mesh,
        in_specs=placed,
        out_specs=(P("ep", "tp"), P("ep", "tp", None)),
        check_vma=False,
    )
```

time: 119 us -> 98.5 us (0.83)
  local copies, waits for them, and re-layouts: 20.3 us -> 1.47 us
    unnamed x39 -> x1, local copies, waits for them, and re-layouts: 19.5 us -> 1.47 us
    pallas_call x1, Pallas kernels: 88.7 us -> 86.8 us  [run_ffn(): pl.pallas_call(ffn_kernel, out_shape=jax.ShapeDtypeStruct((ROWS, HALF), B...]
where the time goes in v2:
time: 98.5 us; the launch traced here: 98.4 us
  Pallas kernels  96.2 us (98%)
  local copies, waits for them, and re-layouts  1.47 us (1%)
    pallas_call x1, Pallas kernels, run_ffn(): pl.pallas_call(ffn_kernel, out_shape=jax.ShapeDtypeStruct((ROWS, HALF), B...  86.8 us
    pallas_call x1, Pallas kernels, run_mixer(): pl.pallas_call(mixer_kernel, out_shape=(jax.ShapeDtypeStruct((256, 4096),...  9.44 us

profile of v2, /device:TPU:0, one launch (start us, length us, event | category | flops | bytes accessed | tf_op | source)
XLA Modules:
  0.0 98.4 jit_solution(17036249573745392741)
XLA Ops:
  0.6 9.4 %mixer.1 = (f32[256,4096]{1,0:T(8,128)}, bf16[32,2048]{1,0:T(8,128)(2,1)}, bf16[16,256]{1,0:T(8,128)(2,1)}) custom-call(bf16[32,2048]{1,0:T(8,128)(2,1)} %stream_hbm.1, f32[1,2048]{1,0:T(1,128)} %bitcast.26, bf16[8,2048]{1,0:T(8,128)(2,1)} %bitcast.24, s32[2,32]{1,0:T(2,128)} %bitcast.29, f32[2,32]{1,0:T(2,128)} %bitcast.30, f32[8]{0:T(128)} %refs_5_.1, ...), custom_call_target="tpu_custom_call" | custom-call | tf_op jit(solution)/shard_map/mixer/pallas_call | solution.py:224
  10.1 86.8 %ffn.1 = bf16[32,1024]{1,0:T(8,128)(2,1)} custom-call(bf16[32,2048]{1,0:T(8,128)(2,1)} %get-tuple-element.5.partial, bf16[16,256]{1,0:T(8,128)(2,1)} %get-tuple-element.6.meta, bf16[32,2048]{1,0:T(8,128)(2,1)} %stream_hbm.1, f32[1,2048]{1,0:T(1,128)} %bitcast.25, f32[1,1024]{1,0:T(1,128)} %bitcast.27, bf16[448,2048]{1,0:T(8,128)(2,1)} %bitcast.18, ...), custom_call_target="tpu_custom_call" | custom-call | tf_op jit(solution)/shard_map/ffn/pallas_call | solution.py:757
  96.9 1.5 %copy.29 = bf16[32,1024]{1,0:T(8,128)(2,1)} copy(bf16[32,1024]{1,0:T(8,128)(2,1)} %ffn.1) | data formatting | bytes 131072

commit v3 on v2

--- a/solution.py
+++ b/solution.py
@@ -274,8 +274,8 @@
     s2,
     *rest,
 ):
-    landed, rest = rest[:18], rest[18:]
-    landing = [(landed[6 * k : 6 * k + 3], landed[6 * k + 3 : 6 * k + 6]) for k in range(3)]
+    landed, rest = rest[:12], rest[12:]
+    landing = [landed[3 * k : 3 * k + 3] for k in range(4)]
     (
     other_partial,
     wide,
@@ -335,12 +335,12 @@
         load.start()
     barrier = pltpu.get_barrier_semaphore()
     for dim in range(3):
-        for shift in (1, 3):
+        for shift in (1, 2, 3):
             pl.semaphore_signal(
                 barrier, inc=1, device_id=neighbour(dim, shift), device_id_type=MESH
             )
     pl.semaphore_signal(barrier, inc=1, device_id=partner, device_id_type=MESH)
-    pl.semaphore_wait(barrier, 7)
+    pl.semaphore_wait(barrier, 10)
 
     def to_partner(src, dst, n):
         return pltpu.make_async_remote_copy(
@@ -403,14 +403,14 @@
     spots = [[[turn(p, k, shift) for shift in range(4)] for k in range(3)] for p in range(3)]
 
     class Ring:
-        def __init__(self, p, k, at, place):
-            self.p, self.k, self.place = p, k, place
-            self.copies = [
-                self.copy(at, ME, None, 1),
-                self.copy(at + 1, ME, None, 3),
-                self.copy(at + 2, LEFT, 0, 1),
-                self.copy(at + 3, RIGHT, 1, 3),
-            ]
+        def __init__(self, p, k, at, place, direct=False):
+            self.p, self.k, self.place, self.direct = p, k, place, direct
+            self.copies = [self.copy(at, ME, None, 1), self.copy(at + 1, ME, None, 3)]
+            if direct:
+                self.copies.append(self.copy(at + 2, ME, None, 2))
+            else:
+                self.copies.append(self.copy(at + 2, LEFT, 0, 1))
+                self.copies.append(self.copy(at + 3, RIGHT, 1, 3))
 
         def copy(self, at, shift, half, to):
             p = self.p
@@ -428,26 +428,33 @@
             )
 
         def start(self):
+            if self.direct:
+                self.copies[2].start()
             self.copies[0].start()
             self.copies[1].start()
 
         def on(self):
             self.copies[0].wait_recv()
-            self.copies[2].start()
+            if not self.direct:
+                self.copies[2].start()
             self.copies[1].wait_recv()
-            self.copies[3].start()
+            if not self.direct:
+                self.copies[3].start()
 
         def end(self):
-            self.copies[2].wait_recv()
-            self.copies[3].wait_recv()
+            for copy in self.copies[2:]:
+                copy.wait_recv()
 
     first, second, blocks, lines = [], [], [], []
     for p in range(3):
         at = 48 * p
         own = [spots[p][k][ME] for k in range(3)]
-        first.append(Ring(p, 0, at, own))
+        first.append(Ring(p, 0, at, own, True))
         second.append(
-            [Ring(p, 1, at + 4 + 4 * u, [spots[p][0][u], None, own[2]]) for u in range(4)]
+            [
+                Ring(p, 1, at + 4 + 4 * u, [spots[p][0][u], None, own[2]], u != ME)
+                for u in range(4)
+            ]
         )
         blocks.append(
             [Ring(p, 2, at + 20 + 4 * u, [spots[p][0][u], own[1], None]) for u in range(4)]
@@ -594,7 +601,7 @@
         slot_weight[slots, :] = dot(slot_tags, pick_weight)
         return carry
 
-    lax.fori_loop(0, GROUPS, pack_group, 0)
+    lax.fori_loop(0, GROUPS, pack_group, 0, unroll=2)
 
     sends = []
     for i in range(2):
@@ -612,30 +619,14 @@
         left_side[g, :, 128:256] = (silu(both[:, 0:128]) * both[:, 128:256]).astype(BF16)
         return carry
 
-    lax.fori_loop(0, GROUPS, dense_group, 0)
+    lax.fori_loop(0, GROUPS, dense_group, 0, unroll=2)
     share = 1.0 / (1.0 + jnp.exp(-mix[...]))
     dd_scaled[0:DENSE, :] = (dd[...].astype(F32) * share).astype(BF16)
-
-    for i in range(2):
-        rows = pl.ds(i * 384, 384)
-        sends[i].wait()
-        back = dot(act[rows, :], ed[...]) + dot(act_other[rows, :], ed_other[...])
-        result[pl.ds(4 * i, 4), 0:SLOTS, :] = back.astype(BF16).reshape(4, SLOTS, HALF)
-
-    def spread_group(g, carry):
-        z, y = g // 2, 2 * lax.rem(g, 2)
-        total = dot(left_side[g], jnp.concatenate([result[g], dd_scaled[...]], axis=0))
-        for p in range(3):
-            cut = total[:, STARTS[p] : STARTS[p] + WIDTHS[p]].astype(BF16)
-            sums[p][z, pl.ds(y, 2)] = cut.reshape(2, 4, ROWS, WIDTHS[p])
-        return carry
-
-    lax.fori_loop(0, GROUPS, spread_group, 0)
 
     class Back:
         def __init__(self, p, k, at, place, slot):
             self.p, self.k, self.place, self.slot = p, k, place, slot
-            self.halves, self.wholes = landing[k][0][p], landing[k][1][p]
+            self.halves, self.wholes = landing[0][p], landing[1][p]
             self.copies = [
                 self.copy(at, FAR, 0, 1, self.halves.at[slot, 0]),
                 self.copy(at + 1, FAR, 1, 3, self.halves.at[slot, 1]),
@@ -671,11 +662,6 @@
             for q in range(3):
                 place[ORDERS[p][q]] = where[q]
             free = [d for d in range(3) if place[d] is None]
-            if not free:
-                rows = pl.ds(16 * half, 16)
-                ref = sums[p].at[tuple(place) + (rows,)]
-                ref[...] = ref[...] + got[self.slot, half]
-                return
             for t in range(2):
                 place[free[0]] = 2 * half + t
                 ref = sums[p].at[tuple(place)]
@@ -689,13 +675,10 @@
             self.add_half(LEFT, 1)
             self.copies[3].start()
 
-        def arrive(self):
+        def end(self):
+            p, got = self.p, self.wholes
             self.copies[2].wait_recv()
             self.copies[3].wait_recv()
-
-        def end(self):
-            p, got = self.p, self.wholes
-            self.arrive()
             where = self.spot(ME)
             place = [None, None, None]
             for q in range(3):
@@ -707,6 +690,43 @@
                 total = ref[...].astype(F32) + got[self.slot, 0, t].astype(F32)
                 ref[...] = (total + got[self.slot, 1, t].astype(F32)).astype(BF16)
 
+    class Straight:
+        def __init__(self, p, k, at, place):
+            self.p, self.k, self.place, self.wholes = p, k, place, landing[2 + k][p]
+            self.copies = [self.copy(at + u - 1, u) for u in (RIGHT, FAR, LEFT)]
+
+        def copy(self, at, u):
+            p = self.p
+            where = list(self.place)
+            where[self.k] = spots[p][self.k][u]
+            return pltpu.make_async_remote_copy(
+                src_ref=cut(sums[p], p, where),
+                dst_ref=self.wholes.at[u - 1],
+                send_sem=rs_send.at[at],
+                recv_sem=rs_recv.at[at],
+                device_id=neighbour(ORDERS[p][self.k], u),
+                device_id_type=MESH,
+            )
+
+        def send(self, u):
+            self.copies[u - 1].start()
+
+        def arrive(self):
+            for copy in self.copies:
+                copy.wait_recv()
+
+        def add(self, first_at):
+            p, got = self.p, self.wholes
+            place = [None, None, None]
+            for q in range(3):
+                place[ORDERS[p][q]] = spots[p][q][ME]
+            place[ORDERS[p][0]] = first_at
+            ref = sums[p].at[tuple(place)]
+            total = ref[...].astype(F32)
+            for n in range(3):
+                total = total + got[n, first_at].astype(F32)
+            ref[...] = total.astype(BF16)
+
     third, middle, last = [], [], []
     for p in parts:
         at = 24 * p
@@ -714,11 +734,29 @@
         third.append(
             [Back(p, 2, at + 4 * u, [None, spots[p][1][u], None], u) for u in range(4)]
         )
-        middle.append(Back(p, 1, at + 16, [None, None, own[2]], 0))
-        last.append(Back(p, 0, at + 20, own, 0))
+        middle.append(Straight(p, 1, at + 16, [None, None, own[2]]))
+        last.append(Straight(p, 0, at + 20, own))
     order = (FAR, LEFT, RIGHT, ME)
-    for u in order:
-        for p in parts:
+    for send in sends:
+        send.wait()
+    for p in parts:
+        cols = slice(STARTS[p], STARTS[p] + WIDTHS[p])
+        for i in range(2):
+            rows = pl.ds(i * 384, 384)
+            back = dot(act[rows, :], ed[:, cols]) + dot(act_other[rows, :], ed_other[:, cols])
+            result[pl.ds(4 * i, 4), 0:SLOTS, cols] = back.astype(BF16).reshape(
+                4, SLOTS, WIDTHS[p]
+            )
+
+        def spread_group(g, carry):
+            z, y = g // 2, 2 * lax.rem(g, 2)
+            right_side = jnp.concatenate([result[g, :, cols], dd_scaled[:, cols]], axis=0)
+            total = dot(left_side[g], right_side).astype(BF16)
+            sums[p][z, pl.ds(y, 2)] = total.reshape(2, 4, ROWS, WIDTHS[p])
+            return carry
+
+        lax.fori_loop(0, GROUPS, spread_group, 0, unroll=2)
+        for u in order:
             third[p][u].start()
     for u in order:
         for p in parts:
@@ -726,22 +764,21 @@
     for u in order:
         for p in parts:
             third[p][u].end()
-            if u == FAR:
-                middle[p].start()
-        if u == RIGHT:
-            for p in parts:
-                middle[p].on()
-    for p in parts:
-        middle[p].end()
-        last[p].start()
-    for p in parts:
-        last[p].on()
+            if u != ME:
+                middle[p].send(u)
+    for p in parts:
+        middle[p].arrive()
+        for u in order:
+            middle[p].add(spots[p][0][u])
+            if u != ME:
+                last[p].send(u)
     for p in parts:
         last[p].arrive()
         got = last[p].wholes
         total = mid[:, pl.ds(pl.multiple_of(own_cols + STARTS[p], 128), WIDTHS[p])]
         total = total + sums[p][here[0], here[1], here[2]].astype(F32)
-        total = total + got[0, 0].astype(F32) + got[0, 1].astype(F32)
+        for n in range(3):
+            total = total + got[n].astype(F32)
         out[:, STARTS[p] : STARTS[p] + WIDTHS[p]] = total.astype(BF16)
     for group in third + [middle, last]:
         for back in group:
@@ -763,12 +800,10 @@
             *[VMEM((4, 4, 4, BLOCK_ROWS[p], WIDTHS[p]), BF16) for p in range(3)],
             *blocks(4, 4, 4, ROWS),
             *blocks(4, 4, 4, ROWS),
-            *blocks(1, 2, 16),
-            *blocks(1, 2, ROWS),
-            *blocks(1, 2, 2, ROWS),
-            *blocks(1, 2, 4, ROWS),
             *blocks(4, 2, 2, ROWS),
             *blocks(4, 2, 4, ROWS),
+            *blocks(3, ROWS),
+            *blocks(3, 4, ROWS),
             VMEM((ROWS, 2 * HALF), BF16),
             VMEM((ROWS, 2 * HALF), BF16),
             VMEM((ROWS, 2 * HALF), F32),

time: 98.5 us -> 89.5 us (0.909)
  Pallas kernels: 96.2 us -> 87.2 us
    pallas_call x1, Pallas kernels: 86.8 us -> 77.8 us  [run_ffn(): pl.pallas_call(ffn_kernel, out_shape=jax.ShapeDtypeStruct((ROWS, HALF), B...]
where the time goes in v3:
time: 89.5 us; the launch traced here: 89.3 us
  Pallas kernels  87.2 us (97%)
  local copies, waits for them, and re-layouts  1.47 us (2%)
    pallas_call x1, Pallas kernels, run_ffn(): pl.pallas_call(ffn_kernel, out_shape=jax.ShapeDtypeStruct((ROWS, HALF), B...  77.8 us
    pallas_call x1, Pallas kernels, run_mixer(): pl.pallas_call(mixer_kernel, out_shape=(jax.ShapeDtypeStruct((256, 4096),...  9.44 us

profile of v3, /device:TPU:0, one launch (start us, length us, event | category | flops | bytes accessed | tf_op | source)
XLA Modules:
  0.0 89.3 jit_solution(11668316452934146207)
XLA Ops:
  0.6 9.4 %mixer.1 = (f32[256,4096]{1,0:T(8,128)}, bf16[32,2048]{1,0:T(8,128)(2,1)}, bf16[16,256]{1,0:T(8,128)(2,1)}) custom-call(bf16[32,2048]{1,0:T(8,128)(2,1)} %stream_hbm.1, f32[1,2048]{1,0:T(1,128)} %bitcast.26, bf16[8,2048]{1,0:T(8,128)(2,1)} %bitcast.24, s32[2,32]{1,0:T(2,128)} %bitcast.29, f32[2,32]{1,0:T(2,128)} %bitcast.30, f32[8]{0:T(128)} %refs_5_.1, ...), custom_call_target="tpu_custom_call" | custom-call | tf_op jit(solution)/shard_map/mixer/pallas_call | solution.py:224
  10.1 77.8 %ffn.1 = bf16[32,1024]{1,0:T(8,128)(2,1)} custom-call(bf16[32,2048]{1,0:T(8,128)(2,1)} %get-tuple-element.5.partial, bf16[16,256]{1,0:T(8,128)(2,1)} %get-tuple-element.6.meta, bf16[32,2048]{1,0:T(8,128)(2,1)} %stream_hbm.1, f32[1,2048]{1,0:T(1,128)} %bitcast.25, f32[1,1024]{1,0:T(1,128)} %bitcast.27, bf16[448,2048]{1,0:T(8,128)(2,1)} %bitcast.18, ...), custom_call_target="tpu_custom_call" | custom-call | tf_op jit(solution)/shard_map/ffn/pallas_call | solution.py:794
  87.9 1.5 %copy.29 = bf16[32,1024]{1,0:T(8,128)(2,1)} copy(bf16[32,1024]{1,0:T(8,128)(2,1)} %ffn.1) | data formatting | bytes 131072

commit v4 on v3

--- a/solution.py
+++ b/solution.py
@@ -445,24 +445,24 @@
             for copy in self.copies[2:]:
                 copy.wait_recv()
 
-    first, second, blocks, lines = [], [], [], []
+    first, second, third_way = [], [], []
     for p in range(3):
-        at = 48 * p
+        at = 84 * p
         own = [spots[p][k][ME] for k in range(3)]
         first.append(Ring(p, 0, at, own, True))
         second.append(
+            [Ring(p, 1, at + 4 + 4 * u, [spots[p][0][u], None, own[2]], True) for u in range(4)]
+        )
+        third_way.append(
             [
-                Ring(p, 1, at + 4 + 4 * u, [spots[p][0][u], None, own[2]], u != ME)
+                [
+                    Ring(p, 2, at + 20 + 16 * u + 4 * v, [spots[p][0][u], spots[p][1][v], None])
+                    for v in range(4)
+                ]
                 for u in range(4)
             ]
         )
-        blocks.append(
-            [Ring(p, 2, at + 20 + 4 * u, [spots[p][0][u], own[1], None]) for u in range(4)]
-        )
-        lines.append(
-            [Ring(p, 2, at + 36 + 4 * (u - 1), [None, spots[p][1][u], None]) for u in (1, 2, 3)]
-        )
-    rings = [first] + second + blocks + lines
+    rings = [first] + second + [row for part in third_way for row in part]
     hand_overs = []
 
     def hand_over(p, n, second_at, third_at):
@@ -479,12 +479,21 @@
         hand_overs.append(copy)
 
     parts = range(3)
+    def launch(*pairs):
+        for p in parts:
+            for u, v in pairs:
+                third_way[p][u][v].start()
+
+    def pass_on(*pairs):
+        for p in parts:
+            for u, v in pairs:
+                third_way[p][u][v].on()
+
     for p in parts:
         first[p].start()
     for p in parts:
         second[p][ME].start()
-    for p in parts:
-        blocks[p][ME].start()
+    launch((ME, ME))
 
     early = [
         to_partner(
@@ -500,25 +509,18 @@
         first[p].on()
         for u in (LEFT, RIGHT):
             second[p][u].start()
-            blocks[p][u].start()
+            third_way[p][u][ME].start()
     for p in parts:
         second[p][ME].on()
-    for p in parts:
-        blocks[p][ME].on()
+    launch((ME, RIGHT), (ME, LEFT))
     for p in parts:
         first[p].end()
         second[p][FAR].start()
-        blocks[p][FAR].start()
-    for p in parts:
-        second[p][LEFT].on()
-        second[p][RIGHT].on()
-    for p in parts:
-        blocks[p][LEFT].on()
-        blocks[p][RIGHT].on()
-    for p in parts:
-        second[p][FAR].on()
-        lines[p][RIGHT - 1].start()
-        lines[p][LEFT - 1].start()
+        third_way[p][FAR][ME].start()
+    for p in parts:
+        second[p][ME].end()
+    launch((ME, FAR))
+    pass_on((ME, ME))
     for ref in (eg, eu, ed, ed_other):
         ref[HIDDEN:HPAD, :] = jnp.zeros((HPAD - HIDDEN, ref.shape[1]), BF16)
     for ref in (dgu, dgu_other):
@@ -528,31 +530,47 @@
     for g in range(GROUPS):
         result[g, SLOTS:128, :] = jnp.zeros((128 - SLOTS, HALF), BF16)
     for p in parts:
-        for u in range(4):
-            second[p][u].end()
-        lines[p][FAR - 1].start()
+        second[p][LEFT].on()
+        second[p][RIGHT].on()
+    launch((LEFT, RIGHT), (RIGHT, RIGHT), (LEFT, LEFT), (RIGHT, LEFT))
+    pass_on((LEFT, ME), (RIGHT, ME), (ME, RIGHT), (ME, LEFT))
+    for p in parts:
+        second[p][LEFT].end()
+        second[p][RIGHT].end()
+    launch((LEFT, FAR), (RIGHT, FAR))
+    for p in parts:
+        second[p][FAR].on()
+    launch((FAR, RIGHT), (FAR, LEFT))
+    for p in parts:
+        second[p][FAR].end()
+    launch((FAR, FAR))
+    pass_on((FAR, ME), (ME, FAR))
+    for p in parts:
         hand_over(p, 0, None, spots[p][2][ME])
-    for p in parts:
-        blocks[p][FAR].on()
         hand_over(p, 1, spots[p][1][ME], spots[p][2][LEFT])
         hand_over(p, 2, spots[p][1][ME], spots[p][2][RIGHT])
-    for n, u in ((3, RIGHT), (6, LEFT), (9, FAR)):
+
+    def finish(v, n):
         for p in parts:
-            lines[p][u - 1].on()
-            hand_over(p, n, spots[p][1][u], spots[p][2][LEFT])
-            hand_over(p, n + 1, spots[p][1][u], spots[p][2][RIGHT])
+            for u in range(4):
+                third_way[p][u][v].end()
+            hand_over(p, n, spots[p][1][v], spots[p][2][FAR])
+
+    def sides(v, n):
         for p in parts:
-            if u == RIGHT:
-                for v in range(4):
-                    blocks[p][v].end()
-                hand_over(p, n + 2, spots[p][1][ME], spots[p][2][FAR])
-            else:
-                done = RIGHT if u == LEFT else LEFT
-                lines[p][done - 1].end()
-                hand_over(p, n + 2, spots[p][1][done], spots[p][2][FAR])
-    for p in parts:
-        lines[p][FAR - 1].end()
-        hand_over(p, 12, spots[p][1][FAR], spots[p][2][FAR])
+            hand_over(p, n, spots[p][1][v], spots[p][2][LEFT])
+            hand_over(p, n + 1, spots[p][1][v], spots[p][2][RIGHT])
+
+    pass_on((LEFT, RIGHT), (RIGHT, RIGHT), (LEFT, LEFT), (RIGHT, LEFT))
+    finish(ME, 3)
+    pass_on((LEFT, FAR), (RIGHT, FAR), (FAR, RIGHT), (FAR, LEFT))
+    sides(RIGHT, 4)
+    sides(LEFT, 6)
+    pass_on((FAR, FAR))
+    sides(FAR, 8)
+    finish(RIGHT, 10)
+    finish(LEFT, 11)
+    finish(FAR, 12)
     for load in loads:
         load.wait()
     for copy in early:
@@ -605,12 +623,11 @@
 
     sends = []
     for i in range(2):
-        rows = pl.ds(i * 384, 384)
-        taken = packed[rows, :]
-        gate = dot_nt(taken, eg[...])
-        up = dot_nt(taken, eu[...])
-        act[rows, :] = (silu(gate) * up * slot_weight[rows, 0:1]).astype(BF16)
-        copy = to_partner(act.at[rows], act_other.at[rows], 4 + i)
+        units = pl.ds(256 * i, 256)
+        gate = dot_nt(packed[...], eg[units, :])
+        up = dot_nt(packed[...], eu[units, :])
+        act[:, units] = (silu(gate) * up * slot_weight[:, 0:1]).astype(BF16)
+        copy = to_partner(act.at[:, units], act_other.at[:, units], 4 + i)
         copy.start()
         sends.append(copy)
 
@@ -741,12 +758,8 @@
         send.wait()
     for p in parts:
         cols = slice(STARTS[p], STARTS[p] + WIDTHS[p])
-        for i in range(2):
-            rows = pl.ds(i * 384, 384)
-            back = dot(act[rows, :], ed[:, cols]) + dot(act_other[rows, :], ed_other[:, cols])
-            result[pl.ds(4 * i, 4), 0:SLOTS, cols] = back.astype(BF16).reshape(
-                4, SLOTS, WIDTHS[p]
-            )
+        back = dot(act[...], ed[:, cols]) + dot(act_other[...], ed_other[:, cols])
+        result[:, 0:SLOTS, cols] = back.astype(BF16).reshape(GROUPS, SLOTS, WIDTHS[p])
 
         def spread_group(g, carry):
             z, y = g // 2, 2 * lax.rem(g, 2)
@@ -822,8 +835,8 @@
             VMEM((GROUPS, GROUP_ROWS, 256), BF16),
             VMEM((GROUPS, 128, HALF), BF16),
             sem((6,)),
-            sem((144,)),
-            sem((144,)),
+            sem((252,)),
+            sem((252,)),
             sem((39,)),
             sem((39,)),
             sem((72,)),

time: 89.5 us -> 90.4 us (1.010)
    pallas_call x1, Pallas kernels: 77.8 us -> 78.7 us  [run_ffn(): pl.pallas_call(ffn_kernel, out_shape=jax.ShapeDtypeStruct((ROWS, HALF), B...]
where the time goes in v4:
time: 90.4 us; the launch traced here: 90.2 us
  Pallas kernels  88.1 us (97%)
  local copies, waits for them, and re-layouts  1.47 us (2%)
    pallas_call x1, Pallas kernels, run_ffn(): pl.pallas_call(ffn_kernel, out_shape=jax.ShapeDtypeStruct((ROWS, HALF), B...  78.7 us
    pallas_call x1, Pallas kernels, run_mixer(): pl.pallas_call(mixer_kernel, out_shape=(jax.ShapeDtypeStruct((256, 4096),...  9.44 us

profile of v4, /device:TPU:0, one launch (start us, length us, event | category | flops | bytes accessed | tf_op | source)
XLA Modules:
  0.0 90.2 jit_solution(2069675301616085014)
XLA Ops:
  0.6 9.4 %mixer.1 = (f32[256,4096]{1,0:T(8,128)}, bf16[32,2048]{1,0:T(8,128)(2,1)}, bf16[16,256]{1,0:T(8,128)(2,1)}) custom-call(bf16[32,2048]{1,0:T(8,128)(2,1)} %stream_hbm.1, f32[1,2048]{1,0:T(1,128)} %bitcast.26, bf16[8,2048]{1,0:T(8,128)(2,1)} %bitcast.24, s32[2,32]{1,0:T(2,128)} %bitcast.29, f32[2,32]{1,0:T(2,128)} %bitcast.30, f32[8]{0:T(128)} %refs_5_.1, ...), custom_call_target="tpu_custom_call" | custom-call | tf_op jit(solution)/shard_map/mixer/pallas_call | solution.py:224
  10.1 78.7 %ffn.1 = bf16[32,1024]{1,0:T(8,128)(2,1)} custom-call(bf16[32,2048]{1,0:T(8,128)(2,1)} %get-tuple-element.5.partial, bf16[16,256]{1,0:T(8,128)(2,1)} %get-tuple-element.6.meta, bf16[32,2048]{1,0:T(8,128)(2,1)} %stream_hbm.1, f32[1,2048]{1,0:T(1,128)} %bitcast.25, f32[1,1024]{1,0:T(1,128)} %bitcast.27, bf16[448,2048]{1,0:T(8,128)(2,1)} %bitcast.18, ...), custom_call_target="tpu_custom_call" | custom-call | tf_op jit(solution)/shard_map/ffn/pallas_call | solution.py:807
  88.8 1.5 %copy.29 = bf16[32,1024]{1,0:T(8,128)(2,1)} copy(bf16[32,1024]{1,0:T(8,128)(2,1)} %ffn.1) | data formatting | bytes 131072

commit v5 on v4

--- a/solution.py
+++ b/solution.py
@@ -27,6 +27,10 @@
 HIDDEN = 448
 HPAD = 512
 DENSE = 88
+WIDTH = 2048
+INNER = 2048
+META = 2560
+CARRY = 2816
 
 WIDTHS = (384, 384, 256)
 STARTS = (0, 384, 768)
@@ -60,10 +64,10 @@
 
 
 def mixer_kernel(*refs):
-    given, refs = refs[:18], refs[18:]
-    state_hbm = given[17]
-    state_out, partial, meta = refs[:3]
-    held, refs = refs[3:20], refs[20:]
+    given, refs = refs[:19], refs[19:]
+    state_hbm = given[18]
+    state_out, carry_hbm = refs[:2]
+    held, refs = refs[2:20], refs[20:]
     (
         stream,
         mixer_gain,
@@ -81,9 +85,12 @@
         map_past,
         inner_gain,
         gate_w,
-        out_w,
+        channel_gain,
+        mix,
     ) = held
-    old, new, dec, write, read, xs_high, xs_low, tmp, y, past, in_sems, sems = refs
+    old, new, dec, write, read, xs_high, xs_low, tmp, y, past, carry, in_sems, sems, out_sems = (
+        refs
+    )
     loads = [
         pltpu.make_async_copy(src, dst, in_sems.at[n])
         for n, (src, dst) in enumerate(zip(given, held))
@@ -103,8 +110,8 @@
         load.start()
     for t in range(CHUNKS):
         load_state(t).start()
-    loads[15].start()
-    loads[16].start()
+    for load in loads[15:]:
+        load.start()
 
     for load in loads[:8]:
         load.wait()
@@ -131,7 +138,8 @@
         == lax.broadcasted_iota(jnp.int32, (ROWS, ROWS), 1)
     ).astype(BF16)
     by_row = dot_nt(eye, table)
-    meta[...] = jnp.concatenate([by_row[0:16], by_row[16:32]], axis=1).astype(BF16)
+    carry[0:16, META : META + 256] = jnp.concatenate([by_row[0:16], by_row[16:32]], axis=1)
+    carry[0:ROWS, 0:WIDTH] = stream[...].astype(F32)
 
     for load in loads[8:11]:
         load.wait()
@@ -193,8 +201,18 @@
 
     lax.fori_loop(0, CHUNKS, chunk_step, 0)
 
-    loads[14].wait()
-    loads[15].wait()
+    for load in loads[14:]:
+        load.wait()
+    carry[ROWS : ROWS + 1, 0:WIDTH] = channel_gain[...]
+    carry[ROWS + 1 : ROWS + 2, 0:HALF] = mix[...]
+    out_parts = []
+    for n, (first, size) in enumerate(((0, WIDTH), (META, 256), (INNER, 512))):
+        where = (pl.ds(0, ROWS + 8), pl.ds(first, size))
+        out_parts.append(
+            pltpu.make_async_copy(carry.at[where], carry_hbm.at[where], out_sems.at[n])
+        )
+    out_parts[0].start()
+    out_parts[1].start()
     gate = silu(dot(normed, gate_w[...]).astype(BF16).astype(F32))
     pieces = []
     for j in range(HEADS // 2):
@@ -207,29 +225,29 @@
         )
     groups = [jnp.concatenate(pieces[2 * g : 2 * g + 2], axis=1) for g in range(2)]
     inner = jnp.concatenate([rms(g) for g in groups], axis=1) * inner_gain[...]
-    loads[16].wait()
-    partial[...] = dot(inner.astype(BF16), out_w[...]).astype(BF16)
+    carry[0:ROWS, INNER : INNER + 512] = inner
+    out_parts[2].start()
+    for part in out_parts:
+        part.wait()
     for t in range(CHUNKS):
         store_state(t).wait()
 
 
 def run_mixer(*given):
-    vmem = pl.BlockSpec(memory_space=VMEM)
     hbm = pl.BlockSpec(memory_space=pltpu.HBM)
     lanes = lambda: VMEM((256, 128), F32)
     held = [
         (pltpu.SMEM if 5 <= n < 8 else VMEM)(v.shape, v.dtype)
-        for n, v in enumerate(given[:17])
+        for n, v in enumerate(given[:18])
     ]
     return pl.pallas_call(
         mixer_kernel,
         out_shape=(
             jax.ShapeDtypeStruct((256, 4096), F32),
-            jax.ShapeDtypeStruct((ROWS, 2 * HALF), BF16),
-            jax.ShapeDtypeStruct((16, 256), BF16),
+            jax.ShapeDtypeStruct((ROWS + 8, CARRY), F32),
         ),
-        in_specs=[hbm] * 18,
-        out_specs=(hbm, vmem, vmem),
+        in_specs=[hbm] * 19,
+        out_specs=(hbm, hbm),
         scratch_shapes=[
             *held,
             VMEM((CHUNKS, 256, CHUNK), F32),
@@ -242,8 +260,10 @@
             lanes(),
             lanes(),
             VMEM((192, 128), F32),
-            pltpu.SemaphoreType.DMA((17,)),
+            VMEM((ROWS + 8, CARRY), F32),
+            pltpu.SemaphoreType.DMA((18,)),
             pltpu.SemaphoreType.DMA((2 * CHUNKS,)),
+            pltpu.SemaphoreType.DMA((3,)),
         ],
         compiler_params=pltpu.CompilerParams(vmem_limit_bytes=67043328),
         name="mixer",
@@ -251,11 +271,8 @@
 
 
 def ffn_kernel(
-    partial,
-    meta,
-    stream_hbm,
-    gain_hbm,
-    mix_hbm,
+    carry_hbm,
+    ow_hbm,
     eg_hbm,
     eu_hbm,
     ed_hbm,
@@ -303,10 +320,10 @@
     rs_recv,
     mi_send,
     mi_recv,
-    stream,
-    gain,
-    mix,
-    small_sem,
+        carry,
+        out_w,
+        partial,
+        small_sem,
     ) = rest
     ep = lax.axis_index("ep")
     core = lax.axis_index("tp")
@@ -327,9 +344,8 @@
     partner = (ep, other)
 
     small = [
-        pltpu.make_async_copy(stream_hbm, stream, small_sem.at[0]),
-        pltpu.make_async_copy(gain_hbm, gain, small_sem.at[1]),
-        pltpu.make_async_copy(mix_hbm, mix, small_sem.at[2]),
+        pltpu.make_async_copy(carry_hbm, carry, small_sem.at[0]),
+        pltpu.make_async_copy(ow_hbm, out_w, small_sem.at[1]),
     ]
     for load in small:
         load.start()
@@ -340,6 +356,10 @@
                 barrier, inc=1, device_id=neighbour(dim, shift), device_id_type=MESH
             )
     pl.semaphore_signal(barrier, inc=1, device_id=partner, device_id_type=MESH)
+    for load in small:
+        load.wait()
+    inner = carry[0:ROWS, INNER : INNER + 512].astype(BF16)
+    partial[...] = dot(inner, out_w[...]).astype(BF16)
     pl.semaphore_wait(barrier, 10)
 
     def to_partner(src, dst, n):
@@ -367,18 +387,18 @@
     for load in loads:
         load.start()
 
-    for load in small:
-        load.wait()
     swap_partial.wait()
     mixed = partial[...].astype(F32) + other_partial[...].astype(F32)
-    hidden = stream[...].astype(F32) + mixed
+    hidden = carry[0:ROWS, 0:WIDTH] + mixed
     mid[...] = hidden
-    wide[...] = (rms(hidden) * gain[...]).astype(BF16)
+    wide[...] = (rms(hidden) * carry[ROWS : ROWS + 1, 0:WIDTH]).astype(BF16)
     here = coords
     for p in range(3):
         cols = pl.ds(pl.multiple_of(own_cols + STARTS[p], 128), WIDTHS[p])
         mine[p][here[0], here[1], here[2], 0:ROWS, :] = wide[:, cols]
-    x2[here[0], here[1], here[2], ROWS : ROWS + 16, :] = meta[...]
+    x2[here[0], here[1], here[2], ROWS : ROWS + 16, :] = carry[0:16, META : META + 256].astype(
+        BF16
+    )
 
     def cut(buf, p, where, half=None, rows=None):
         index = [None, None, None]
@@ -456,7 +476,13 @@
         third_way.append(
             [
                 [
-                    Ring(p, 2, at + 20 + 16 * u + 4 * v, [spots[p][0][u], spots[p][1][v], None])
+                    Ring(
+                        p,
+                        2,
+                        at + 20 + 16 * u + 4 * v,
+                        [spots[p][0][u], spots[p][1][v], None],
+                        FAR in (u, v) and ME not in (u, v),
+                    )
                     for v in range(4)
                 ]
                 for u in range(4)
@@ -571,17 +597,6 @@
     finish(RIGHT, 10)
     finish(LEFT, 11)
     finish(FAR, 12)
-    for load in loads:
-        load.wait()
-    for copy in early:
-        copy.wait()
-    for group in rings:
-        for ring in group:
-            for copy in ring.copies:
-                copy.wait_send()
-    for copy in hand_overs:
-        copy.wait()
-
     pick_row = lax.broadcasted_iota(jnp.int32, (128, 128), 0)
     pick_rank = (pick_row == expert).astype(F32).astype(BF16)
     pick_weight = (
@@ -612,14 +627,31 @@
         used = table[:, 0:SLOTS]
         slots = pl.ds(pl.multiple_of(g * SLOTS, SLOTS), SLOTS)
         packed[slots, pl.ds(own_cols, HALF)] = dot_tn(used, group_of(mine, g)).astype(BF16)
+        slot_tags = dot_tn(used, tags).astype(BF16)
+        slot_weight[slots, :] = dot(slot_tags, pick_weight)
+        return carry
+
+    lax.fori_loop(0, GROUPS, pack_group, 0, unroll=2)
+    for load in loads:
+        load.wait()
+    for copy in early:
+        copy.wait()
+    for group in rings:
+        for ring in group:
+            for copy in ring.copies:
+                copy.wait_send()
+    for copy in hand_overs:
+        copy.wait()
+
+    def pack_other(g, carry):
+        used = left_side[g, :, 0:SLOTS]
+        slots = pl.ds(pl.multiple_of(g * SLOTS, SLOTS), SLOTS)
         packed[slots, pl.ds(other_cols, HALF)] = dot_tn(used, group_of(theirs, g)).astype(
             BF16
         )
-        slot_tags = dot_tn(used, tags).astype(BF16)
-        slot_weight[slots, :] = dot(slot_tags, pick_weight)
         return carry
 
-    lax.fori_loop(0, GROUPS, pack_group, 0, unroll=2)
+    lax.fori_loop(0, GROUPS, pack_other, 0, unroll=2)
 
     sends = []
     for i in range(2):
@@ -637,7 +669,7 @@
         return carry
 
     lax.fori_loop(0, GROUPS, dense_group, 0, unroll=2)
-    share = 1.0 / (1.0 + jnp.exp(-mix[...]))
+    share = 1.0 / (1.0 + jnp.exp(-carry[ROWS + 1 : ROWS + 2, 0:HALF]))
     dd_scaled[0:DENSE, :] = (dd[...].astype(F32) * share).astype(BF16)
 
     class Back:
@@ -799,7 +831,7 @@
                 copy.wait_send()
 
 
-def run_ffn(partial, meta, stream, gain, mix, eg, eu, ed, dg, du, dd):
+def run_ffn(carry, out_w, eg, eu, ed, dg, du, dd):
     vmem = pl.BlockSpec(memory_space=VMEM)
     hbm = pl.BlockSpec(memory_space=pltpu.HBM)
     blocks = lambda *lead: [VMEM((*lead, WIDTHS[p]), BF16) for p in range(3)]
@@ -807,7 +839,7 @@
     return pl.pallas_call(
         ffn_kernel,
         out_shape=jax.ShapeDtypeStruct((ROWS, HALF), BF16),
-        in_specs=[vmem] * 2 + [hbm] * 9,
+        in_specs=[hbm] * 8,
         out_specs=vmem,
         scratch_shapes=[
             *[VMEM((4, 4, 4, BLOCK_ROWS[p], WIDTHS[p]), BF16) for p in range(3)],
@@ -843,16 +875,16 @@
             sem((72,)),
             sem((6,)),
             sem((6,)),
+            VMEM((ROWS + 8, CARRY), F32),
+            VMEM((512, 2 * HALF), BF16),
             VMEM((ROWS, 2 * HALF), BF16),
-            VMEM((1, 2 * HALF), F32),
-            VMEM((1, HALF), F32),
-            sem((3,)),
+            sem((2,)),
         ],
         compiler_params=pltpu.CompilerParams(
             collective_id=0, has_side_effects=True, vmem_limit_bytes=67043328
         ),
         name="ffn",
-    )(partial, meta, stream, gain, mix, eg, eu, ed, dg, du, dd)
+    )(carry, out_w, eg, eu, ed, dg, du, dd)
 
 
 def local(
@@ -883,7 +915,7 @@
     dense_down,
     dense_mix,
 ):
-    state_out, partial, meta = run_mixer(
+    state_out, carry = run_mixer(
         stream,
         mixer_gain.reshape(1, -1),
         step_proj.T,
@@ -900,15 +932,13 @@
         jnp.transpose(map_past, (0, 2, 1, 3)).reshape(192, 128),
         inner_gain.reshape(1, -1),
         gate_proj,
-        mixer_out,
+        channel_gain.reshape(1, -1),
+        dense_mix.reshape(1, -1),
         head_state.reshape(256, 4096),
     )
     out = run_ffn(
-        partial,
-        meta,
-        stream,
-        channel_gain.reshape(1, -1),
-        dense_mix.reshape(1, -1),
+        carry,
+        mixer_out,
         expert_gate.T,
         expert_up.T,
         expert_down,

time: 90.4 us -> 88.4 us (0.978)
  Pallas kernels: 88.1 us -> 86.1 us
    pallas_call x1, Pallas kernels: 78.7 us -> 77.3 us  [run_ffn(): pl.pallas_call(ffn_kernel, out_shape=jax.ShapeDtypeStruct((ROWS, HALF), B...]
where the time goes in v5:
time: 88.4 us; the launch traced here: 88.2 us
  Pallas kernels  86.1 us (97%)
  local copies, waits for them, and re-layouts  1.47 us (2%)
    pallas_call x1, Pallas kernels, run_ffn(): pl.pallas_call(ffn_kernel, out_shape=jax.ShapeDtypeStruct((ROWS, HALF), B...  77.3 us
    pallas_call x1, Pallas kernels, run_mixer(): pl.pallas_call(mixer_kernel, out_shape=(jax.ShapeDtypeStruct((256, 4096),...  8.82 us

profile of v5, /device:TPU:0, one launch (start us, length us, event | category | flops | bytes accessed | tf_op | source)
XLA Modules:
  0.0 88.2 jit_solution(13126276662575991921)
XLA Ops:
  0.6 8.8 %mixer.1 = (f32[256,4096]{1,0:T(8,128)}, f32[40,2816]{1,0:T(8,128)}) custom-call(bf16[32,2048]{1,0:T(8,128)(2,1)} %refs_0_.1, f32[1,2048]{1,0:T(1,128)} %bitcast.25, bf16[8,2048]{1,0:T(8,128)(2,1)} %bitcast.24, s32[2,32]{1,0:T(2,128)} %bitcast.29, f32[2,32]{1,0:T(2,128)} %bitcast.30, f32[8]{0:T(128)} %refs_5_.1, f32[8]{0:T(128)} %refs_6_.1, f32[8]{0:T(128)} %refs_7_.1, ...), custom_call_target="tpu_custom_call" | custom-call | tf_op jit(solution)/shard_map/mixer/pallas_call | solution.py:243
  9.5 77.3 %ffn.1 = bf16[32,1024]{1,0:T(8,128)(2,1)} custom-call(f32[40,2816]{1,0:T(8,128)} %get-tuple-element.4.carry_hbm, bf16[512,2048]{1,0:T(8,128)(2,1)} %ow_hbm.1, bf16[448,2048]{1,0:T(8,128)(2,1)} %bitcast.18, bf16[448,2048]{1,0:T(8,128)(2,1)} %bitcast.19, bf16[448,2048]{1,0:T(8,128)(2,1)} %ed_hbm.1, bf16[88,1024]{1,0:T(8,128)(2,1)} %bitcast.20, ...), custom_call_target="tpu_custom_call" | custom-call | tf_op jit(solution)/shard_map/ffn/pallas_call | solution.py:839
  86.7 1.5 %copy.29 = bf16[32,1024]{1,0:T(8,128)(2,1)} copy(bf16[32,1024]{1,0:T(8,128)(2,1)} %ffn.1) | data formatting | bytes 131072

commit v6 on v5

--- a/solution.py
+++ b/solution.py
@@ -199,7 +199,7 @@
         y[...] += dot_nt(high, spread) + dot_nt(low, spread)
         return carry
 
-    lax.fori_loop(0, CHUNKS, chunk_step, 0)
+    lax.fori_loop(0, CHUNKS, chunk_step, 0, unroll=4)
 
     for load in loads[14:]:
         load.wait()
@@ -631,7 +631,7 @@
         slot_weight[slots, :] = dot(slot_tags, pick_weight)
         return carry
 
-    lax.fori_loop(0, GROUPS, pack_group, 0, unroll=2)
+    lax.fori_loop(0, GROUPS, pack_group, 0, unroll=8)
     for load in loads:
         load.wait()
     for copy in early:
@@ -651,7 +651,7 @@
         )
         return carry
 
-    lax.fori_loop(0, GROUPS, pack_other, 0, unroll=2)
+    lax.fori_loop(0, GROUPS, pack_other, 0, unroll=8)
 
     sends = []
     for i in range(2):
@@ -668,7 +668,7 @@
         left_side[g, :, 128:256] = (silu(both[:, 0:128]) * both[:, 128:256]).astype(BF16)
         return carry
 
-    lax.fori_loop(0, GROUPS, dense_group, 0, unroll=2)
+    lax.fori_loop(0, GROUPS, dense_group, 0, unroll=8)
     share = 1.0 / (1.0 + jnp.exp(-carry[ROWS + 1 : ROWS + 2, 0:HALF]))
     dd_scaled[0:DENSE, :] = (dd[...].astype(F32) * share).astype(BF16)
 
@@ -790,8 +790,10 @@
         send.wait()
     for p in parts:
         cols = slice(STARTS[p], STARTS[p] + WIDTHS[p])
-        back = dot(act[...], ed[:, cols]) + dot(act_other[...], ed_other[:, cols])
-        result[:, 0:SLOTS, cols] = back.astype(BF16).reshape(GROUPS, SLOTS, WIDTHS[p])
+        for n in ((0, 1), (2,), (3,))[p]:
+            some = slice(256 * n, 256 * n + 256)
+            back = dot(act[...], ed[:, some]) + dot(act_other[...], ed_other[:, some])
+            result[:, 0:SLOTS, some] = back.astype(BF16).reshape(GROUPS, SLOTS, 256)
 
         def spread_group(g, carry):
             z, y = g // 2, 2 * lax.rem(g, 2)
@@ -800,7 +802,7 @@
             sums[p][z, pl.ds(y, 2)] = total.reshape(2, 4, ROWS, WIDTHS[p])
             return carry
 
-        lax.fori_loop(0, GROUPS, spread_group, 0, unroll=2)
+        lax.fori_loop(0, GROUPS, spread_group, 0, unroll=8)
         for u in order:
             third[p][u].start()
     for u in order:

time: 88.4 us -> 86.1 us (0.974)
  Pallas kernels: 86.1 us -> 83.7 us
    pallas_call x1, Pallas kernels: 77.3 us -> 74.7 us  [run_ffn(): pl.pallas_call(ffn_kernel, out_shape=jax.ShapeDtypeStruct((ROWS, HALF), B...]
where the time goes in v6:
time: 86.1 us; the launch traced here: 85.9 us
  Pallas kernels  83.7 us (97%)
  local copies, waits for them, and re-layouts  1.47 us (2%)
    pallas_call x1, Pallas kernels, run_ffn(): pl.pallas_call(ffn_kernel, out_shape=jax.ShapeDtypeStruct((ROWS, HALF), B...  74.7 us
    pallas_call x1, Pallas kernels, run_mixer(): pl.pallas_call(mixer_kernel, out_shape=(jax.ShapeDtypeStruct((256, 4096),...  9 us

profile of v6, /device:TPU:0, one launch (start us, length us, event | category | flops | bytes accessed | tf_op | source)
XLA Modules:
  0.0 85.9 jit_solution(8001325732171392991)
XLA Ops:
  0.6 9.0 %mixer.1 = (f32[256,4096]{1,0:T(8,128)}, f32[40,2816]{1,0:T(8,128)}) custom-call(bf16[32,2048]{1,0:T(8,128)(2,1)} %refs_0_.1, f32[1,2048]{1,0:T(1,128)} %bitcast.25, bf16[8,2048]{1,0:T(8,128)(2,1)} %bitcast.24, s32[2,32]{1,0:T(2,128)} %bitcast.29, f32[2,32]{1,0:T(2,128)} %bitcast.30, f32[8]{0:T(128)} %refs_5_.1, f32[8]{0:T(128)} %refs_6_.1, f32[8]{0:T(128)} %refs_7_.1, ...), custom_call_target="tpu_custom_call" | custom-call | tf_op jit(solution)/shard_map/mixer/pallas_call | solution.py:243
  9.7 74.7 %ffn.1 = bf16[32,1024]{1,0:T(8,128)(2,1)} custom-call(f32[40,2816]{1,0:T(8,128)} %get-tuple-element.4.carry_hbm, bf16[512,2048]{1,0:T(8,128)(2,1)} %ow_hbm.1, bf16[448,2048]{1,0:T(8,128)(2,1)} %bitcast.18, bf16[448,2048]{1,0:T(8,128)(2,1)} %bitcast.19, bf16[448,2048]{1,0:T(8,128)(2,1)} %ed_hbm.1, bf16[88,1024]{1,0:T(8,128)(2,1)} %bitcast.20, ...), custom_call_target="tpu_custom_call" | custom-call | tf_op jit(solution)/shard_map/ffn/pallas_call | solution.py:841
  84.4 1.5 %copy.29 = bf16[32,1024]{1,0:T(8,128)(2,1)} copy(bf16[32,1024]{1,0:T(8,128)(2,1)} %ffn.1) | data formatting | bytes 131072

commit v7 on v6

--- a/solution.py
+++ b/solution.py
@@ -28,9 +28,8 @@
 HPAD = 512
 DENSE = 88
 WIDTH = 2048
-INNER = 2048
-META = 2560
-CARRY = 2816
+META = 2048
+CARRY = 2304
 
 WIDTHS = (384, 384, 256)
 STARTS = (0, 384, 768)
@@ -64,10 +63,10 @@
 
 
 def mixer_kernel(*refs):
-    given, refs = refs[:19], refs[19:]
-    state_hbm = given[18]
-    state_out, carry_hbm = refs[:2]
-    held, refs = refs[2:20], refs[20:]
+    given, refs = refs[:20], refs[20:]
+    state_hbm = given[19]
+    state_out, carry_hbm, partial_hbm = refs[:3]
+    held, refs = refs[3:22], refs[22:]
     (
         stream,
         mixer_gain,
@@ -87,10 +86,9 @@
         gate_w,
         channel_gain,
         mix,
+        out_w,
     ) = held
-    old, new, dec, write, read, xs_high, xs_low, tmp, y, past, carry, in_sems, sems, out_sems = (
-        refs
-    )
+    old, new, dec, write, read, xs, tmp, y, past, carry, partial, in_sems, sems, out_sems = refs
     loads = [
         pltpu.make_async_copy(src, dst, in_sems.at[n])
         for n, (src, dst) in enumerate(zip(given, held))
@@ -180,33 +178,33 @@
         write[rows, :] = write_by_group[h // 4]
         read[rows, :] = read_by_group[h // 4]
     high, low = split(tmp[...])
-    xs_high[...] = high
-    xs_low[...] = low
+    xs[:, 0:128] = high
+    xs[:, 128:256] = low
     y[...] = jnp.zeros_like(y)
 
-    slot = lax.broadcasted_iota(jnp.int32, (128, CHUNK), 0) % 64
-    place = lax.broadcasted_iota(jnp.int32, (128, CHUNK), 1) // 64
+    slot = lax.broadcasted_iota(jnp.int32, (256, CHUNK), 0) % 64
+    place = lax.broadcasted_iota(jnp.int32, (256, CHUNK), 1) // 64
 
     def chunk_step(t, carry):
         spread = (slot == place + 8 * t).astype(F32).astype(BF16)
         load_state(t).wait()
-        values = dot(xs_high[...], spread) + dot(xs_low[...], spread)
+        values = dot(xs[...], spread)
         wide = lambda ref: jnp.concatenate([ref[...]] * (CHUNK // 128), axis=1)
         fresh = wide(dec) * old[t] + values * wide(write)
         new[t] = fresh
         store_state(t).start()
-        high, low = split(fresh * wide(read))
-        y[...] += dot_nt(high, spread) + dot_nt(low, spread)
+        both = dot_nt(jnp.concatenate(split(fresh * wide(read)), axis=0), spread[0:128])
+        y[...] += both[0:256] + both[256:512]
         return carry
 
     lax.fori_loop(0, CHUNKS, chunk_step, 0, unroll=4)
 
-    for load in loads[14:]:
+    for load in loads[14:18]:
         load.wait()
     carry[ROWS : ROWS + 1, 0:WIDTH] = channel_gain[...]
     carry[ROWS + 1 : ROWS + 2, 0:HALF] = mix[...]
     out_parts = []
-    for n, (first, size) in enumerate(((0, WIDTH), (META, 256), (INNER, 512))):
+    for n, (first, size) in enumerate(((0, WIDTH), (META, 256))):
         where = (pl.ds(0, ROWS + 8), pl.ds(first, size))
         out_parts.append(
             pltpu.make_async_copy(carry.at[where], carry_hbm.at[where], out_sems.at[n])
@@ -225,7 +223,9 @@
         )
     groups = [jnp.concatenate(pieces[2 * g : 2 * g + 2], axis=1) for g in range(2)]
     inner = jnp.concatenate([rms(g) for g in groups], axis=1) * inner_gain[...]
-    carry[0:ROWS, INNER : INNER + 512] = inner
+    loads[18].wait()
+    partial[...] = dot(inner.astype(BF16), out_w[...]).astype(BF16)
+    out_parts.append(pltpu.make_async_copy(partial, partial_hbm, out_sems.at[2]))
     out_parts[2].start()
     for part in out_parts:
         part.wait()
@@ -238,16 +238,17 @@
     lanes = lambda: VMEM((256, 128), F32)
     held = [
         (pltpu.SMEM if 5 <= n < 8 else VMEM)(v.shape, v.dtype)
-        for n, v in enumerate(given[:18])
+        for n, v in enumerate(given[:19])
     ]
     return pl.pallas_call(
         mixer_kernel,
         out_shape=(
             jax.ShapeDtypeStruct((256, 4096), F32),
             jax.ShapeDtypeStruct((ROWS + 8, CARRY), F32),
+            jax.ShapeDtypeStruct((ROWS, 2 * HALF), BF16),
         ),
-        in_specs=[hbm] * 19,
-        out_specs=(hbm, hbm),
+        in_specs=[hbm] * 20,
+        out_specs=(hbm, hbm, hbm),
         scratch_shapes=[
             *held,
             VMEM((CHUNKS, 256, CHUNK), F32),
@@ -255,13 +256,13 @@
             lanes(),
             lanes(),
             lanes(),
-            VMEM((256, 128), BF16),
-            VMEM((256, 128), BF16),
+            VMEM((256, 256), BF16),
             lanes(),
             lanes(),
             VMEM((192, 128), F32),
             VMEM((ROWS + 8, CARRY), F32),
-            pltpu.SemaphoreType.DMA((18,)),
+            VMEM((ROWS, 2 * HALF), BF16),
+            pltpu.SemaphoreType.DMA((19,)),
             pltpu.SemaphoreType.DMA((2 * CHUNKS,)),
             pltpu.SemaphoreType.DMA((3,)),
         ],
@@ -272,7 +273,7 @@
 
 def ffn_kernel(
     carry_hbm,
-    ow_hbm,
+    partial_hbm,
     eg_hbm,
     eu_hbm,
     ed_hbm,
@@ -321,7 +322,6 @@
     mi_send,
     mi_recv,
         carry,
-        out_w,
         partial,
         small_sem,
     ) = rest
@@ -344,8 +344,8 @@
     partner = (ep, other)
 
     small = [
-        pltpu.make_async_copy(carry_hbm, carry, small_sem.at[0]),
-        pltpu.make_async_copy(ow_hbm, out_w, small_sem.at[1]),
+        pltpu.make_async_copy(partial_hbm, partial, small_sem.at[0]),
+        pltpu.make_async_copy(carry_hbm, carry, small_sem.at[1]),
     ]
     for load in small:
         load.start()
@@ -356,10 +356,7 @@
                 barrier, inc=1, device_id=neighbour(dim, shift), device_id_type=MESH
             )
     pl.semaphore_signal(barrier, inc=1, device_id=partner, device_id_type=MESH)
-    for load in small:
-        load.wait()
-    inner = carry[0:ROWS, INNER : INNER + 512].astype(BF16)
-    partial[...] = dot(inner, out_w[...]).astype(BF16)
+    small[0].wait()
     pl.semaphore_wait(barrier, 10)
 
     def to_partner(src, dst, n):
@@ -387,6 +384,7 @@
     for load in loads:
         load.start()
 
+    small[1].wait()
     swap_partial.wait()
     mixed = partial[...].astype(F32) + other_partial[...].astype(F32)
     hidden = carry[0:ROWS, 0:WIDTH] + mixed
@@ -833,7 +831,7 @@
                 copy.wait_send()
 
 
-def run_ffn(carry, out_w, eg, eu, ed, dg, du, dd):
+def run_ffn(carry, partial, eg, eu, ed, dg, du, dd):
     vmem = pl.BlockSpec(memory_space=VMEM)
     hbm = pl.BlockSpec(memory_space=pltpu.HBM)
     blocks = lambda *lead: [VMEM((*lead, WIDTHS[p]), BF16) for p in range(3)]
@@ -878,7 +876,6 @@
             sem((6,)),
             sem((6,)),
             VMEM((ROWS + 8, CARRY), F32),
-            VMEM((512, 2 * HALF), BF16),
             VMEM((ROWS, 2 * HALF), BF16),
             sem((2,)),
         ],
@@ -886,7 +883,7 @@
             collective_id=0, has_side_effects=True, vmem_limit_bytes=67043328
         ),
         name="ffn",
-    )(carry, out_w, eg, eu, ed, dg, du, dd)
+    )(carry, partial, eg, eu, ed, dg, du, dd)
 
 
 def local(
@@ -917,7 +914,7 @@
     dense_down,
     dense_mix,
 ):
-    state_out, carry = run_mixer(
+    state_out, carry, partial = run_mixer(
         stream,
         mixer_gain.reshape(1, -1),
         step_proj.T,
@@ -936,11 +933,12 @@
         gate_proj,
         channel_gain.reshape(1, -1),
         dense_mix.reshape(1, -1),
+        mixer_out,
         head_state.reshape(256, 4096),
     )
     out = run_ffn(
         carry,
-        mixer_out,
+        partial,
         expert_gate.T,
         expert_up.T,
         expert_down,

time: 86.1 us -> 85.7 us (level)
  no operation moved by 1% of the time
where the time goes in v7:
time: 85.7 us; the launch traced here: 85.6 us
  Pallas kernels  83.4 us (97%)
  local copies, waits for them, and re-layouts  1.47 us (2%)
    pallas_call x1, Pallas kernels, run_ffn(): pl.pallas_call(ffn_kernel, out_shape=jax.ShapeDtypeStruct((ROWS, HALF), B...  74.7 us
    pallas_call x1, Pallas kernels, run_mixer(): pl.pallas_call(mixer_kernel, out_shape=(jax.ShapeDtypeStruct((256, 4096),...  8.7 us

profile of v7, /device:TPU:0, one launch (start us, length us, event | category | flops | bytes accessed | tf_op | source)
XLA Modules:
  0.0 85.6 jit_solution(1997230459150089982)
XLA Ops:
  0.6 8.7 %mixer.1 = (f32[256,4096]{1,0:T(8,128)}, f32[40,2304]{1,0:T(8,128)}, bf16[32,2048]{1,0:T(8,128)(2,1)}) custom-call(bf16[32,2048]{1,0:T(8,128)(2,1)} %refs_0_.1, f32[1,2048]{1,0:T(1,128)} %bitcast.25, bf16[8,2048]{1,0:T(8,128)(2,1)} %bitcast.24, s32[2,32]{1,0:T(2,128)} %bitcast.29, f32[2,32]{1,0:T(2,128)} %bitcast.30, f32[8]{0:T(128)} %refs_5_.1, f32[8]{0:T(128)} %refs_6_.1, ...), custom_call_target="tpu_custom_call" | custom-call | tf_op jit(solution)/shard_map/mixer/pallas_call | solution.py:243
  9.3 74.7 %ffn.1 = bf16[32,1024]{1,0:T(8,128)(2,1)} custom-call(f32[40,2304]{1,0:T(8,128)} %get-tuple-element.5.carry_hbm, bf16[32,2048]{1,0:T(8,128)(2,1)} %get-tuple-element.6.partial_hbm, bf16[448,2048]{1,0:T(8,128)(2,1)} %bitcast.18, bf16[448,2048]{1,0:T(8,128)(2,1)} %bitcast.19, bf16[448,2048]{1,0:T(8,128)(2,1)} %ed_hbm.1, bf16[88,1024]{1,0:T(8,128)(2,1)} %bitcast.20, ...), custom_call_target="tpu_custom_call" | custom-call | tf_op jit(solution)/shard_map/ffn/pallas_call | solution.py:839
  84.1 1.5 %copy.29 = bf16[32,1024]{1,0:T(8,128)(2,1)} copy(bf16[32,1024]{1,0:T(8,128)(2,1)} %ffn.1) | data formatting | bytes 131072

commit v8 on v7

--- a/solution.py
+++ b/solution.py
@@ -104,12 +104,11 @@
             new.at[t], state_out.at[:, cols], sems.at[CHUNKS + t]
         )
 
-    for load in loads[:15]:
+    for load in loads[:18]:
         load.start()
     for t in range(CHUNKS):
         load_state(t).start()
-    for load in loads[15:]:
-        load.start()
+    loads[18].start()
 
     for load in loads[:8]:
         load.wait()
@@ -182,23 +181,6 @@
     xs[:, 128:256] = low
     y[...] = jnp.zeros_like(y)
 
-    slot = lax.broadcasted_iota(jnp.int32, (256, CHUNK), 0) % 64
-    place = lax.broadcasted_iota(jnp.int32, (256, CHUNK), 1) // 64
-
-    def chunk_step(t, carry):
-        spread = (slot == place + 8 * t).astype(F32).astype(BF16)
-        load_state(t).wait()
-        values = dot(xs[...], spread)
-        wide = lambda ref: jnp.concatenate([ref[...]] * (CHUNK // 128), axis=1)
-        fresh = wide(dec) * old[t] + values * wide(write)
-        new[t] = fresh
-        store_state(t).start()
-        both = dot_nt(jnp.concatenate(split(fresh * wide(read)), axis=0), spread[0:128])
-        y[...] += both[0:256] + both[256:512]
-        return carry
-
-    lax.fori_loop(0, CHUNKS, chunk_step, 0, unroll=4)
-
     for load in loads[14:18]:
         load.wait()
     carry[ROWS : ROWS + 1, 0:WIDTH] = channel_gain[...]
@@ -212,6 +194,23 @@
     out_parts[0].start()
     out_parts[1].start()
     gate = silu(dot(normed, gate_w[...]).astype(BF16).astype(F32))
+    slot = lax.broadcasted_iota(jnp.int32, (256, CHUNK), 0) % 64
+    place = lax.broadcasted_iota(jnp.int32, (256, CHUNK), 1) // 64
+
+    def chunk_step(t, carry):
+        spread = (slot == place + 8 * t).astype(F32).astype(BF16)
+        load_state(t).wait()
+        values = dot(xs[...], spread)
+        wide = lambda ref: jnp.concatenate([ref[...]] * (CHUNK // 128), axis=1)
+        fresh = wide(dec) * old[t] + values * wide(write)
+        new[t] = fresh
+        store_state(t).start()
+        both = dot_nt(jnp.concatenate(split(fresh * wide(read)), axis=0), spread[0:128])
+        y[...] += both[0:256] + both[256:512]
+        return carry
+
+    lax.fori_loop(0, CHUNKS, chunk_step, 0, unroll=4)
+
     pieces = []
     for j in range(HEADS // 2):
         even = y[pl.ds(2 * j, ROWS, stride=HEADS), :]
@@ -323,6 +322,8 @@
     mi_recv,
         carry,
         partial,
+        gate_own,
+        up_own,
         small_sem,
     ) = rest
     ep = lax.axis_index("ep")
@@ -632,12 +633,14 @@
     lax.fori_loop(0, GROUPS, pack_group, 0, unroll=8)
     for load in loads:
         load.wait()
+    own = pl.ds(own_cols, HALF)
+    rest_cols = pl.ds(other_cols, HALF)
+    for i in range(2):
+        units = pl.ds(256 * i, 256)
+        gate_own[:, units] = dot_nt(packed[:, own], eg[units, own])
+        up_own[:, units] = dot_nt(packed[:, own], eu[units, own])
     for copy in early:
         copy.wait()
-    for group in rings:
-        for ring in group:
-            for copy in ring.copies:
-                copy.wait_send()
     for copy in hand_overs:
         copy.wait()
 
@@ -654,8 +657,8 @@
     sends = []
     for i in range(2):
         units = pl.ds(256 * i, 256)
-        gate = dot_nt(packed[...], eg[units, :])
-        up = dot_nt(packed[...], eu[units, :])
+        gate = gate_own[:, units] + dot_nt(packed[:, rest_cols], eg[units, rest_cols])
+        up = up_own[:, units] + dot_nt(packed[:, rest_cols], eu[units, rest_cols])
         act[:, units] = (silu(gate) * up * slot_weight[:, 0:1]).astype(BF16)
         copy = to_partner(act.at[:, units], act_other.at[:, units], 4 + i)
         copy.start()
@@ -825,9 +828,9 @@
         for n in range(3):
             total = total + got[n].astype(F32)
         out[:, STARTS[p] : STARTS[p] + WIDTHS[p]] = total.astype(BF16)
-    for group in third + [middle, last]:
-        for back in group:
-            for copy in back.copies:
+    for group in third + [middle, last] + rings:
+        for sender in group:
+            for copy in sender.copies:
                 copy.wait_send()
 
 
@@ -877,6 +880,8 @@
             sem((6,)),
             VMEM((ROWS + 8, CARRY), F32),
             VMEM((ROWS, 2 * HALF), BF16),
+            VMEM((GROUPS * SLOTS, HPAD), F32),
+            VMEM((GROUPS * SLOTS, HPAD), F32),
             sem((2,)),
         ],
         compiler_params=pltpu.CompilerParams(

time: 85.7 us -> 87.7 us (1.023)
  Pallas kernels: 83.4 us -> 85.4 us
    pallas_call x1, Pallas kernels: 74.7 us -> 75.8 us  [run_ffn(): pl.pallas_call(ffn_kernel, out_shape=jax.ShapeDtypeStruct((ROWS, HALF), B...]
where the time goes in v8:
time: 87.7 us; the launch traced here: 87.5 us
  Pallas kernels  85.4 us (97%)
  local copies, waits for them, and re-layouts  1.47 us (2%)
    pallas_call x1, Pallas kernels, run_ffn(): pl.pallas_call(ffn_kernel, out_shape=jax.ShapeDtypeStruct((ROWS, HALF), B...  75.8 us
    pallas_call x1, Pallas kernels, run_mixer(): pl.pallas_call(mixer_kernel, out_shape=(jax.ShapeDtypeStruct((256, 4096),...  9.52 us

profile of v8, /device:TPU:0, one launch (start us, length us, event | category | flops | bytes accessed | tf_op | source)
XLA Modules:
  0.0 87.5 jit_solution(10481839691702533387)
XLA Ops:
  0.6 9.5 %mixer.1 = (f32[256,4096]{1,0:T(8,128)}, f32[40,2304]{1,0:T(8,128)}, bf16[32,2048]{1,0:T(8,128)(2,1)}) custom-call(bf16[32,2048]{1,0:T(8,128)(2,1)} %refs_0_.1, f32[1,2048]{1,0:T(1,128)} %bitcast.25, bf16[8,2048]{1,0:T(8,128)(2,1)} %bitcast.24, s32[2,32]{1,0:T(2,128)} %bitcast.29, f32[2,32]{1,0:T(2,128)} %bitcast.30, f32[8]{0:T(128)} %refs_5_.1, f32[8]{0:T(128)} %refs_6_.1, ...), custom_call_target="tpu_custom_call" | custom-call | tf_op jit(solution)/shard_map/mixer/pallas_call | solution.py:242
  10.2 75.8 %ffn.1 = bf16[32,1024]{1,0:T(8,128)(2,1)} custom-call(f32[40,2304]{1,0:T(8,128)} %get-tuple-element.5.carry_hbm, bf16[32,2048]{1,0:T(8,128)(2,1)} %get-tuple-element.6.partial_hbm, bf16[448,2048]{1,0:T(8,128)(2,1)} %bitcast.18, bf16[448,2048]{1,0:T(8,128)(2,1)} %bitcast.19, bf16[448,2048]{1,0:T(8,128)(2,1)} %ed_hbm.1, bf16[88,1024]{1,0:T(8,128)(2,1)} %bitcast.20, ...), custom_call_target="tpu_custom_call" | custom-call | tf_op jit(solution)/shard_map/ffn/pallas_call | solution.py:842
  86.0 1.5 %copy.29 = bf16[32,1024]{1,0:T(8,128)(2,1)} copy(bf16[32,1024]{1,0:T(8,128)(2,1)} %ffn.1) | data formatting | bytes 131072

commit v9 on v7

--- a/solution.py
+++ b/solution.py
@@ -323,6 +323,8 @@
     mi_recv,
         carry,
         partial,
+        gate_own,
+        up_own,
         small_sem,
     ) = rest
     ep = lax.axis_index("ep")
@@ -632,12 +634,14 @@
     lax.fori_loop(0, GROUPS, pack_group, 0, unroll=8)
     for load in loads:
         load.wait()
+    own = pl.ds(own_cols, HALF)
+    rest_cols = pl.ds(other_cols, HALF)
+    for i in range(2):
+        units = pl.ds(256 * i, 256)
+        gate_own[:, units] = dot_nt(packed[:, own], eg[units, own])
+        up_own[:, units] = dot_nt(packed[:, own], eu[units, own])
     for copy in early:
         copy.wait()
-    for group in rings:
-        for ring in group:
-            for copy in ring.copies:
-                copy.wait_send()
     for copy in hand_overs:
         copy.wait()
 
@@ -654,8 +658,8 @@
     sends = []
     for i in range(2):
         units = pl.ds(256 * i, 256)
-        gate = dot_nt(packed[...], eg[units, :])
-        up = dot_nt(packed[...], eu[units, :])
+        gate = gate_own[:, units] + dot_nt(packed[:, rest_cols], eg[units, rest_cols])
+        up = up_own[:, units] + dot_nt(packed[:, rest_cols], eu[units, rest_cols])
         act[:, units] = (silu(gate) * up * slot_weight[:, 0:1]).astype(BF16)
         copy = to_partner(act.at[:, units], act_other.at[:, units], 4 + i)
         copy.start()
@@ -825,9 +829,9 @@
         for n in range(3):
             total = total + got[n].astype(F32)
         out[:, STARTS[p] : STARTS[p] + WIDTHS[p]] = total.astype(BF16)
-    for group in third + [middle, last]:
-        for back in group:
-            for copy in back.copies:
+    for group in third + [middle, last] + rings:
+        for sender in group:
+            for copy in sender.copies:
                 copy.wait_send()
 
 
@@ -877,6 +881,8 @@
             sem((6,)),
             VMEM((ROWS + 8, CARRY), F32),
             VMEM((ROWS, 2 * HALF), BF16),
+            VMEM((GROUPS * SLOTS, HPAD), F32),
+            VMEM((GROUPS * SLOTS, HPAD), F32),
             sem((2,)),
         ],
         compiler_params=pltpu.CompilerParams(

time: 85.7 us -> 86.8 us (1.013)
  Pallas kernels: 83.4 us -> 84.5 us
    pallas_call x1, Pallas kernels: 74.7 us -> 75.8 us  [run_ffn(): pl.pallas_call(ffn_kernel, out_shape=jax.ShapeDtypeStruct((ROWS, HALF), B...]
where the time goes in v9:
time: 86.8 us; the launch traced here: 86.7 us
  Pallas kernels  84.5 us (97%)
  local copies, waits for them, and re-layouts  1.47 us (2%)
    pallas_call x1, Pallas kernels, run_ffn(): pl.pallas_call(ffn_kernel, out_shape=jax.ShapeDtypeStruct((ROWS, HALF), B...  75.8 us
    pallas_call x1, Pallas kernels, run_mixer(): pl.pallas_call(mixer_kernel, out_shape=(jax.ShapeDtypeStruct((256, 4096),...  8.7 us

profile of v9, /device:TPU:0, one launch (start us, length us, event | category | flops | bytes accessed | tf_op | source)
XLA Modules:
  0.0 86.7 jit_solution(17825346763941815700)
XLA Ops:
  0.6 8.7 %mixer.1 = (f32[256,4096]{1,0:T(8,128)}, f32[40,2304]{1,0:T(8,128)}, bf16[32,2048]{1,0:T(8,128)(2,1)}) custom-call(bf16[32,2048]{1,0:T(8,128)(2,1)} %refs_0_.1, f32[1,2048]{1,0:T(1,128)} %bitcast.25, bf16[8,2048]{1,0:T(8,128)(2,1)} %bitcast.24, s32[2,32]{1,0:T(2,128)} %bitcast.29, f32[2,32]{1,0:T(2,128)} %bitcast.30, f32[8]{0:T(128)} %refs_5_.1, f32[8]{0:T(128)} %refs_6_.1, ...), custom_call_target="tpu_custom_call" | custom-call | tf_op jit(solution)/shard_map/mixer/pallas_call | solution.py:243
  9.3 75.8 %ffn.1 = bf16[32,1024]{1,0:T(8,128)(2,1)} custom-call(f32[40,2304]{1,0:T(8,128)} %get-tuple-element.5.carry_hbm, bf16[32,2048]{1,0:T(8,128)(2,1)} %get-tuple-element.6.partial_hbm, bf16[448,2048]{1,0:T(8,128)(2,1)} %bitcast.18, bf16[448,2048]{1,0:T(8,128)(2,1)} %bitcast.19, bf16[448,2048]{1,0:T(8,128)(2,1)} %ed_hbm.1, bf16[88,1024]{1,0:T(8,128)(2,1)} %bitcast.20, ...), custom_call_target="tpu_custom_call" | custom-call | tf_op jit(solution)/shard_map/ffn/pallas_call | solution.py:843
  85.2 1.5 %copy.29 = bf16[32,1024]{1,0:T(8,128)(2,1)} copy(bf16[32,1024]{1,0:T(8,128)(2,1)} %ffn.1) | data formatting | bytes 131072

commit v10 on v7

--- a/solution.py
+++ b/solution.py
@@ -469,7 +469,7 @@
         own = [spots[p][k][ME] for k in range(3)]
         first.append(Ring(p, 0, at, own, True))
         second.append(
-            [Ring(p, 1, at + 4 + 4 * u, [spots[p][0][u], None, own[2]], True) for u in range(4)]
+            [Ring(p, 1, at + 4 + 4 * u, [spots[p][0][u], None, own[2]], u != ME) for u in range(4)]
         )
         third_way.append(
             [
@@ -634,10 +634,6 @@
         load.wait()
     for copy in early:
         copy.wait()
-    for group in rings:
-        for ring in group:
-            for copy in ring.copies:
-                copy.wait_send()
     for copy in hand_overs:
         copy.wait()
 
@@ -825,9 +821,9 @@
         for n in range(3):
             total = total + got[n].astype(F32)
         out[:, STARTS[p] : STARTS[p] + WIDTHS[p]] = total.astype(BF16)
-    for group in third + [middle, last]:
-        for back in group:
-            for copy in back.copies:
+    for group in third + [middle, last] + rings:
+        for sender in group:
+            for copy in sender.copies:
                 copy.wait_send()
 
 

time: 85.7 us -> 86.2 us (level)
  no operation moved by 1% of the time
where the time goes in v10:
time: 86.2 us; the launch traced here: 86 us
  Pallas kernels  83.9 us (97%)
  local copies, waits for them, and re-layouts  1.47 us (2%)
    pallas_call x1, Pallas kernels, run_ffn(): pl.pallas_call(ffn_kernel, out_shape=jax.ShapeDtypeStruct((ROWS, HALF), B...  75.2 us
    pallas_call x1, Pallas kernels, run_mixer(): pl.pallas_call(mixer_kernel, out_shape=(jax.ShapeDtypeStruct((256, 4096),...  8.7 us

profile of v10, /device:TPU:0, one launch (start us, length us, event | category | flops | bytes accessed | tf_op | source)
XLA Modules:
  0.0 86.0 jit_solution(916411495481499340)
XLA Ops:
  0.6 8.7 %mixer.1 = (f32[256,4096]{1,0:T(8,128)}, f32[40,2304]{1,0:T(8,128)}, bf16[32,2048]{1,0:T(8,128)(2,1)}) custom-call(bf16[32,2048]{1,0:T(8,128)(2,1)} %refs_0_.1, f32[1,2048]{1,0:T(1,128)} %bitcast.25, bf16[8,2048]{1,0:T(8,128)(2,1)} %bitcast.24, s32[2,32]{1,0:T(2,128)} %bitcast.29, f32[2,32]{1,0:T(2,128)} %bitcast.30, f32[8]{0:T(128)} %refs_5_.1, f32[8]{0:T(128)} %refs_6_.1, ...), custom_call_target="tpu_custom_call" | custom-call | tf_op jit(solution)/shard_map/mixer/pallas_call | solution.py:243
  9.3 75.2 %ffn.1 = bf16[32,1024]{1,0:T(8,128)(2,1)} custom-call(f32[40,2304]{1,0:T(8,128)} %get-tuple-element.5.carry_hbm, bf16[32,2048]{1,0:T(8,128)(2,1)} %get-tuple-element.6.partial_hbm, bf16[448,2048]{1,0:T(8,128)(2,1)} %bitcast.18, bf16[448,2048]{1,0:T(8,128)(2,1)} %bitcast.19, bf16[448,2048]{1,0:T(8,128)(2,1)} %ed_hbm.1, bf16[88,1024]{1,0:T(8,128)(2,1)} %bitcast.20, ...), custom_call_target="tpu_custom_call" | custom-call | tf_op jit(solution)/shard_map/ffn/pallas_call | solution.py:835
  84.5 1.5 %copy.29 = bf16[32,1024]{1,0:T(8,128)(2,1)} copy(bf16[32,1024]{1,0:T(8,128)(2,1)} %ffn.1) | data formatting | bytes 131072
